TPU v7x, 32 devices: a whole 2x2x4 slice. The times are simulated.
32 devices in a mesh: grp: 2 (over y), sp: 4 (over z), tp: 4 (over x, core).
Axes of the slice: x: 2, y: 2, z: 4, core: 2. Of those that a mesh axis runs over, the one named last changes fastest.
Arguments:
- query_first: bfloat16 [1536, 512], P(('grp', 'sp'), 'tp'), parts along dimension 0, may hold values from -172 to 172
- key_first: bfloat16 [1536, 512], P(('grp', 'sp'), 'tp'), parts along dimension 0, may hold values from -7.8 to 7.8
- query_second: bfloat16 [1536, 1024], P(('grp', 'sp'), 'tp'), parts along dimension 0, may hold values from -172 to 172
- key_second: bfloat16 [1536, 1024], P(('grp', 'sp'), 'tp'), parts along dimension 0, may hold values from -7.8 to 7.8
- values: bfloat16 [1536, 2, 512], P(('grp', 'sp'), None, 'tp'), parts along dimension 0, may hold values from -6 to 6
- lambdas: float32 [2, 4], P(None, 'tp'), may hold values from 0.3 to 0.8
- residual: bfloat16 [1536, 2048], P(('grp', 'sp'), 'tp'), parts along dimension 0, may hold values from -130 to 130
- norm_gain: bfloat16 [2048], P('tp'), may hold values from 0.099609375 to 1.8984375
- out_weight: bfloat16 [2, 512, 2048], P(None, 'tp'), may hold values from -0.1875 to 0.1875
- gate_weight: bfloat16 [2048, 5632], P('sp', 'tp'), may hold values from -0.125 to 0.125
- up_weight: bfloat16 [2048, 5632], P('sp', 'tp'), may hold values from -0.125 to 0.125
- down_weight: bfloat16 [5632, 2048], P('tp', 'sp'), may hold values from -0.078125 to 0.078125
Outputs:
- layer_out: bfloat16 [1536, 2048], P(('grp', 'sp'), 'tp'), parts along dimension 0
There are 2 independent parts, one for each index of `grp`. A program takes and returns all parts, laid end to end along the dimension named above; an argument that names none is the same for every part. Nothing has to cross between parts.
All inputs are finite; a program needn't handle non-finite values.
Results may differ from a plain program's by a relative error of at most 0.0065.
Values may be sent and summed in bfloat16 or wider, within the bound.
A program may use at most 128 MiB of HBM per device.

v0:
```python
import functools

import jax
import jax.numpy as jnp
from jax import lax
from jax.experimental import pallas as pl
from jax.experimental.pallas import tpu as pltpu
from jax.sharding import PartitionSpec as P

D = 2048


def per_device(
    query_first,
    key_first,
    query_second,
    key_second,
    values,
    lambdas,
    residual,
    norm_gain,
    out_weight,
    gate_weight,
    up_weight,
    down_weight,
):
    tok_rows = query_first.shape[0]
    heads_here = lambdas.shape[1]
    width_first = query_first.shape[1] // (2 * heads_here)
    width_second = query_second.shape[1] // (2 * heads_here)
    value_size = values.shape[2] // heads_here
    offset = lax.axis_index("sp") * tok_rows
    query_pos = offset + lax.broadcasted_iota(jnp.int32, (tok_rows, 1), 0)
    query_groups = (
        query_first.reshape(tok_rows, heads_here, 2, width_first),
        query_second.reshape(tok_rows, heads_here, 2, width_second),
    )
    key_widths = (width_first, width_second)
    start_state = (
        jnp.full((heads_here, 2, tok_rows, 1), -1e30, jnp.float32),
        jnp.zeros((heads_here, 2, tok_rows, 1), jnp.float32),
        jnp.zeros((heads_here, 2, tok_rows, value_size), jnp.float32),
    )
    states = (start_state, start_state)
    pieces = (
        lax.all_gather(key_first, "sp", axis=0, tiled=True),
        lax.all_gather(key_second, "sp", axis=0, tiled=True),
        lax.all_gather(values, "sp", axis=0, tiled=True),
    )
    piece_rows = pieces[0].shape[0]
    key_pos = lax.broadcasted_iota(jnp.int32, (1, piece_rows), 1)
    allowed = key_pos <= query_pos
    value_rows = pieces[2].reshape(piece_rows, 2, heads_here, value_size)
    results = []
    for group_idx in range(2):
        key_width = key_widths[group_idx]
        key_part = pieces[group_idx].reshape(piece_rows, heads_here, 2, key_width)
        scores = jnp.einsum(
            "qhmd,khmd->hmqk", query_groups[group_idx], key_part, preferred_element_type=jnp.float32
        ) * key_width ** (-0.5)
        scores = jnp.where(allowed, scores, -1e30)
        running, totals, weighted = states[group_idx]
        new_peak = jnp.maximum(running, jnp.max(scores, axis=-1, keepdims=True))
        weights = jnp.where(allowed, jnp.exp(scores - new_peak), 0.0)
        totals = jnp.sum(weights, axis=-1, keepdims=True)
        weighted = jnp.einsum(
            "hmqk,khe->hmqe",
            weights.astype(jnp.bfloat16),
            value_rows[:, group_idx],
            preferred_element_type=jnp.float32,
        )
        results.append((new_peak, totals, weighted))
    states = (results[0], results[1])
    map_out = jnp.stack([states[0][2] / states[0][1], states[1][2] / states[1][1]])
    differ = map_out[:, :, 0] - lambdas[:, :, None, None] * map_out[:, :, 1]
    head_scale = lax.rsqrt(jnp.mean(differ * differ, axis=-1, keepdims=True) + 1e-06)
    attended = (0.8 * differ * head_scale).astype(jnp.bfloat16)
    projection = out_weight.reshape(2, heads_here, value_size, out_weight.shape[2])
    mixed_part = jnp.einsum(
        "ghqe,gher->qr", attended, projection, preferred_element_type=jnp.float32
    )
    mixed = lax.psum_scatter(
        mixed_part.astype(jnp.bfloat16), "tp", scatter_dimension=1, tiled=True
    ).astype(jnp.float32)
    stream = residual.astype(jnp.float32) + mixed
    squares = lax.psum(jnp.sum(stream * stream, axis=1), "tp")
    row_scale = lax.rsqrt(squares[:, None] / D + 1e-06)
    normed = (stream * row_scale * norm_gain.astype(jnp.float32)).astype(jnp.bfloat16)
    full_rows = lax.all_gather(normed, "tp", axis=1, tiled=True)
    pieces = (
        lax.all_gather(gate_weight, "sp", axis=0, tiled=True),
        lax.all_gather(up_weight, "sp", axis=0, tiled=True),
    )
    gate = jnp.dot(full_rows, pieces[0], preferred_element_type=jnp.float32)
    up_part = jnp.dot(full_rows, pieces[1], preferred_element_type=jnp.float32)
    hidden = (jax.nn.silu(gate) * up_part).astype(jnp.bfloat16)
    partial_out = jnp.dot(
        hidden,
        lax.all_gather(down_weight, "sp", axis=1, tiled=True),
        preferred_element_type=jnp.float32,
    )
    ffn = lax.psum_scatter(
        partial_out.astype(jnp.bfloat16), "tp", scatter_dimension=1, tiled=True
    ).astype(jnp.float32)
    return (stream + 0.5 * ffn).astype(jnp.bfloat16)


def flip(index, bits):
    bit = 1
    while bit <= bits:
        if (bits // bit) % 2:
            index = index + bit - 2 * bit * ((index // bit) % 2)
        bit *= 2
    return index


def nt_dot(a, b):
    return lax.dot_general(a, b, (((1,), (1,)), ((), ())), preferred_element_type=jnp.float32)


def dot(a, b):
    return jnp.dot(a, b, preferred_element_type=jnp.float32)


def layer_kernel(
    sp_count,
    widths,
    q1_ref,
    q2_ref,
    k1_ref,
    k2_ref,
    v_ref,
    lam_ref,
    residual_ref,
    gain_ref,
    proj_hbm,
    gate_ref,
    up_ref,
    down_ref,
    out_ref,
    k1b,
    k2b,
    vb,
    proj_ref,
    peak,
    total,
    acc,
    wg,
    wu,
    wd,
    mp,
    rsb,
    stream,
    act,
    gains,
    hid,
    c1,
    c1r,
    po,
    c2,
    c2r,
    c3,
    c3r,
    kv_ss,
    kv_rs,
    w_ss,
    w_rs,
    f_ss,
    f_rs,
    own_sem,
    g_ss,
    g_rs,
    rs_ss,
    rs_rs,
    az_ss,
    az_rs,
    ax_ss,
    ax_rs,
    ac_ss,
    ac_rs,
    c_ss,
    c_rs,
):
    s = lax.axis_index("sp")
    t = lax.axis_index("tp")
    y = lax.axis_index("grp")
    rows, blk = residual_ref.shape
    cols = wg.shape[2]
    hidden_all = gate_ref.shape[1]
    value_size = acc.shape[2]
    xpeer, cpeer, dpeer = flip(t, 2), flip(t, 1), flip(t, 3)
    others = range(1, sp_count)

    def remote(src, dst, ssem, rsem, **where):
        return pltpu.make_async_remote_copy(
            src_ref=src,
            dst_ref=dst,
            send_sem=ssem,
            recv_sem=rsem,
            device_id=where,
            device_id_type=pl.DeviceIdType.MESH,
        )

    barrier = pltpu.get_barrier_semaphore()
    for k in others:
        pl.semaphore_signal(barrier, inc=1, device_id={"sp": flip(s, k)}, device_id_type=pl.DeviceIdType.MESH)
        pl.semaphore_signal(barrier, inc=1, device_id={"tp": flip(t, k)}, device_id_type=pl.DeviceIdType.MESH)
    pl.semaphore_signal(barrier, inc=1, device_id={"grp": 1 - y}, device_id_type=pl.DeviceIdType.MESH)
    pl.semaphore_wait(barrier, 2 * (sp_count - 1) + 1)

    sends = []

    right, left = lax.rem(s + 1, sp_count), lax.rem(s + sp_count - 1, sp_count)
    has_right, has_left = s + 1 < sp_count, s > 0

    def kv_copy(back):
        pairs = ((k1_ref, k1b), (k2_ref, k2b), (v_ref, vb))
        return [
            remote(dst.at[back] if back else src, dst.at[back + 1], kv_ss.at[i, back], kv_rs.at[i, back + 1], sp=right)
            for i, (src, dst) in enumerate(pairs)
        ]

    kv_copies = {back: kv_copy(back) for back in range(sp_count - 1)}

    def kv_send(back):
        @pl.when(jnp.logical_and(has_right, s >= back))
        def _():
            for copy in kv_copies[back]:
                copy.start()

    kv_send(0)

    half_d = wg.shape[1] // 2
    half_c = cols // 2
    extra = sp_count * cols - hidden_all
    half_last = (cols - extra) // 2
    d_half = pl.ds(pl.multiple_of(y * half_d, half_d), half_d)
    last = sp_count - 1

    def w_copy(kind, k, source, target, short):
        src, dst = ((gate_ref, wg), (up_ref, wu), (down_ref, wd))[kind]
        begin = hidden_all - cols + extra if short else pl.multiple_of(target * cols, 128)
        skip, size = (extra, cols - extra) if short else (0, cols)
        if kind < 2:
            piece = src.at[d_half, pl.ds(begin, size)]
            place = dst.at[source, d_half, pl.ds(skip, size)]
        else:
            part = y * (size // 2)
            piece = src.at[pl.ds(pl.multiple_of(begin + part, 64), size // 2), :]
            place = dst.at[source, pl.ds(pl.multiple_of(skip + part, 64), size // 2)]
        return remote(piece, place, w_ss.at[kind, k], w_rs.at[kind, k], sp=flip(s, k)), place

    def f_copy(kind, k, short):
        _, place = w_copy(kind, k, flip(s, k), s, short)
        return remote(place, place, f_ss.at[kind, k], f_rs.at[kind, k], grp=1 - y)

    def either(test, action):
        pl.when(test)(lambda: action(True))
        pl.when(jnp.logical_not(test))(lambda: action(False))

    def send_weights(kinds, rightward):
        for k in others:

            def go(short, k=k):
                for kind in kinds:
                    w_copy(kind, k, s, flip(s, k), short)[0].start()

            target = flip(s, k)
            if rightward:
                pl.when(target == last)(functools.partial(go, True))
                pl.when(jnp.logical_and(target > s, target != last))(functools.partial(go, False))
            else:
                pl.when(target < s)(functools.partial(go, False))

    @pl.when(s == last)
    def _():
        wg[:, :, :extra] = jnp.zeros((sp_count, wg.shape[1], extra), jnp.bfloat16)
        wu[:, :, :extra] = jnp.zeros((sp_count, wg.shape[1], extra), jnp.bfloat16)
        wd[:, :extra, :] = jnp.zeros((sp_count, extra, blk), jnp.bfloat16)

    send_weights((0, 1), False)
    proj_copy = pltpu.make_async_copy(proj_hbm, proj_ref, own_sem.at[3])
    proj_copy.start()
    def own_copy(kind, short):
        src, dst = ((gate_ref, wg), (up_ref, wu), (down_ref, wd))[kind]
        begin = hidden_all - cols + extra if short else pl.multiple_of(s * cols, 128)
        skip, size = (extra, cols - extra) if short else (0, cols)
        if kind < 2:
            return pltpu.make_async_copy(src.at[:, pl.ds(begin, size)], dst.at[s, :, pl.ds(skip, size)], own_sem.at[kind])
        return pltpu.make_async_copy(src.at[pl.ds(begin, size), :], dst.at[s, pl.ds(skip, size)], own_sem.at[kind])

    def start_own(short):
        for kind in range(3):
            own_copy(kind, short).start()

    either(s == last, start_own)

    gains[t] = jnp.broadcast_to(gain_ref[...].reshape(1, blk), gains.shape[1:])
    gain_copies = []
    for k in others:
        copy = remote(gains.at[t], gains.at[t], g_ss.at[k], g_rs.at[k], tp=flip(t, k))
        copy.start()
        gain_copies.append(copy)
        sends.append(copy)

    q_refs = (q1_ref, q2_ref)
    lane = lax.broadcasted_iota(jnp.int32, (1, 2 * widths[0]), 1)

    def block(keys, v, diagonal):
        for group in range(2):
            width = widths[group]
            values = v[:, group, :]
            for m in range(2):
                if width % 128:
                    span = slice(0, 2 * width)
                    queries = q_refs[group][:, span]
                    queries = jnp.where(lane // width == m, queries.astype(jnp.float32), 0.0).astype(jnp.bfloat16)
                else:
                    span = slice(m * width, (m + 1) * width)
                    queries = q_refs[group][:, span]
                scores = nt_dot(queries, keys[group][:, span]) * width ** (-0.5)
                state = 2 * group + m
                if diagonal:
                    allowed = lax.broadcasted_iota(jnp.int32, (rows, rows), 1) <= lax.broadcasted_iota(
                        jnp.int32, (rows, rows), 0
                    )
                    scores = jnp.where(allowed, scores, -1e30)
                    top = jnp.max(scores, axis=1, keepdims=True)
                    weights = jnp.exp(scores - top)
                    peak[state] = top
                    total[state] = jnp.sum(weights, axis=1, keepdims=True)
                    acc[state] = dot(weights.astype(jnp.bfloat16), values)
                else:
                    before = peak[state]
                    top = jnp.maximum(before, jnp.max(scores, axis=1, keepdims=True))
                    fade = jnp.exp(before - top)
                    weights = jnp.exp(scores - top)
                    peak[state] = top
                    total[state] = total[state] * fade + jnp.sum(weights, axis=1, keepdims=True)
                    acc[state] = acc[state] * fade + dot(weights.astype(jnp.bfloat16), values)

    block((k1_ref, k2_ref), v_ref, True)
    for back in others:

        @pl.when(s >= back)
        def _(back=back):
            for copy in kv_copies[back - 1]:
                copy.wait_recv()

        if back in kv_copies:
            kv_send(back)
        if back == sp_count - 2:
            send_weights((0, 1), True)

        @pl.when(s >= back)
        def _(back=back):
            block((k1b.at[back], k2b.at[back]), vb.at[back], False)

    proj_copy.wait()
    attended = []
    for group in range(2):
        first = acc[2 * group] / total[2 * group]
        second = acc[2 * group + 1] / total[2 * group + 1]
        differ = first - lam_ref[0, group] * second
        scale = lax.rsqrt(jnp.mean(differ * differ, axis=1, keepdims=True) + 1e-06)
        attended.append((0.8 * differ * scale).astype(jnp.bfloat16))

    def project(owner):
        columns = pl.ds(pl.multiple_of(owner * blk, blk), blk)
        return dot(attended[0], proj_ref[0, :, columns]) + dot(attended[1], proj_ref[1, :, columns])

    def hand_over(kinds, k):
        def go(short):
            for kind in kinds:
                w_copy(kind, k, flip(s, k), s, short)[0].wait_recv()
                f_copy(kind, k, short).start()

        either(s == last, go)

    rs_copies = {}
    for k in (2, 3, 1):
        mp[k] = project(flip(t, k)).astype(jnp.bfloat16)
        rs_copies[k] = remote(mp.at[k], rsb.at[k], rs_ss.at[k], rs_rs.at[k], tp=flip(t, k))
        rs_copies[k].start()
        sends.append(rs_copies[k])
    mixed = project(t)
    hand_over((0, 1), 1)
    for k in (1, 2, 3):
        rs_copies[k].wait_recv()
        mixed = mixed + rsb[k].astype(jnp.float32)
    stream[...] = residual_ref[...].astype(jnp.float32) + mixed
    act[t, s] = stream[...].astype(jnp.bfloat16)

    ax, ac0, ac1 = {}, {}, {}
    for k in range(sp_count):
        row = flip(s, k)
        ax[k] = remote(act.at[t, row], act.at[t, row], ax_ss.at[k], ax_rs.at[k], tp=xpeer)
        ac0[k] = remote(act.at[t, row], act.at[t, row], ac_ss.at[0, k], ac_rs.at[0, k], tp=cpeer)
        ac1[k] = remote(act.at[xpeer, row], act.at[xpeer, row], ac_ss.at[1, k], ac_rs.at[1, k], tp=cpeer)

    def along_line(k, action):
        row = flip(s, k)
        piece = act.at[t, row]

        @pl.when(jnp.logical_and(has_right, row <= s))
        def _():
            action(remote(piece, piece, az_ss.at[0, row], az_rs.at[row], sp=right))

        @pl.when(jnp.logical_and(has_left, row >= s))
        def _():
            action(remote(piece, piece, az_ss.at[1, row], az_rs.at[row], sp=left))

    along_line(0, lambda copy: copy.start())
    send_weights((2,), True)
    send_weights((2,), False)

    def pass_on(k):
        if k:
            row = flip(s, k)
            piece = act.at[t, row]
            remote(piece, piece, az_ss.at[0, row], az_rs.at[row], sp=right).wait_recv()
            along_line(k, lambda copy: copy.start())
        ax[k].start()
        ac0[k].start()

    def pass_inside(k):
        ax[k].wait_recv()
        ac1[k].start()

    def await_weights(kinds):
        def go(short):
            for kind in kinds:
                own_copy(kind, short).wait()
                for k in others:
                    f_copy(kind, k, short).wait_recv()

        either(s == last, go)

    turns = (0, 1, 3, 2)
    pass_on(0)
    for at, k in enumerate(turns[1:]):
        if at + 2 < sp_count:
            hand_over((0, 1), at + 2)
        pass_on(k)
        pass_inside(turns[at])
    pass_inside(turns[-1])

    for copy in gain_copies:
        copy.wait_recv()
    await_weights((0, 1))
    column = jnp.minimum(s * cols, hidden_all - cols) + lax.broadcasted_iota(jnp.int32, (1, cols), 1)
    mine = column >= s * cols

    def hidden_of(k):
        row = flip(s, k)
        ac0[k].wait_recv()
        ac1[k].wait_recv()
        squares = jnp.zeros((rows, 1), jnp.float32)
        for part in range(sp_count):
            piece = act[part, row].astype(jnp.float32)
            squares = squares + jnp.sum(piece * piece, axis=1, keepdims=True)
        scale = lax.rsqrt(squares / (sp_count * blk) + 1e-06)
        gate = jnp.zeros((rows, cols), jnp.float32)
        up = jnp.zeros((rows, cols), jnp.float32)
        for part in range(sp_count):
            gain = gains[part, 0:1, :].astype(jnp.float32)
            normed = (act[part, row].astype(jnp.float32) * scale * gain).astype(jnp.bfloat16)
            gate = gate + dot(normed, wg[part])
            up = up + dot(normed, wu[part])
        hidden = gate / (1.0 + jnp.exp(-gate)) * up
        hid[k] = jnp.where(mine, hidden, 0.0).astype(jnp.bfloat16)

    r1, r2, r3 = {}, {}, {}
    for k in range(sp_count):
        r1[k] = remote(c1.at[k], c1r.at[k], c_ss.at[0, k], c_rs.at[0, k], tp=cpeer)
        r2[k] = remote(c2.at[k], c2r.at[k], c_ss.at[1, k], c_rs.at[1, k], tp=xpeer)
        if k:
            r3[k] = remote(c3.at[k], c3r.at[k], c_ss.at[2, k], c_rs.at[2, k], sp=flip(s, k))

    def down_of(k):
        hidden = hid[k]
        c1[k, 0] = dot(hidden, wd[cpeer]).astype(jnp.bfloat16)
        c1[k, 1] = dot(hidden, wd[dpeer]).astype(jnp.bfloat16)
        r1[k].start()
        po[k, 1] = dot(hidden, wd[xpeer])
        po[k, 0] = dot(hidden, wd[t])

    def across(k):
        r1[k].wait_recv()
        c2[k] = (po[k, 1] + c1r[k, 1].astype(jnp.float32)).astype(jnp.bfloat16)
        r2[k].start()

    def along(k):
        r2[k].wait_recv()
        result = po[k, 0] + c1r[k, 0].astype(jnp.float32) + c2r[k].astype(jnp.float32)
        if k:
            c3[k] = result.astype(jnp.bfloat16)
            r3[k].start()
        else:
            po[0, 0] = result

    for at, k in enumerate(turns):
        hidden_of(k)
        if at + 1 < sp_count:
            hand_over((2,), at + 1)
    await_weights((2,))
    order = (3, 2, 1, 0)
    for at, k in enumerate(order):
        down_of(k)
        if at >= 1:
            across(order[at - 1])
        if at >= 2:
            along(order[at - 2])
    across(order[-1])
    along(order[-2])
    along(order[-1])

    ffn = po[0, 0]
    for k in order[:-1]:
        r3[k].wait_recv()
        ffn = ffn + c3r[k].astype(jnp.float32)
    out_ref[...] = (stream[...] + 0.5 * ffn).astype(jnp.bfloat16)

    for back in kv_copies:

        @pl.when(jnp.logical_and(has_right, s >= back))
        def _(back=back):
            for copy in kv_copies[back]:
                copy.wait_send()

    def finish():
        for k in others:

            def go(short, k=k):
                for kind in range(3):
                    w_copy(kind, k, s, flip(s, k), short)[0].wait_send()

            either(flip(s, k) == last, go)

        def gone(short):
            for k in others:
                for kind in range(3):
                    f_copy(kind, k, short).wait_send()

        either(s == last, gone)

    finish()
    for k in range(sp_count):
        along_line(k, lambda copy: copy.wait_send())
    for copies in (ax, ac0, ac1, r1, r2, r3):
        sends.extend(copies.values())
    for copy in sends:
        copy.wait_send()


def fits(axes, query_first, values, lambdas, residual, gate_weight):
    sp, tp = axes["sp"], axes["tp"]
    rows, blk = residual.shape
    depth, hidden_all = gate_weight.shape
    if axes["grp"] != 2 or sp != tp or tp != 4 or lambdas.shape[1] != 1:
        return False
    if depth != blk or blk % 128 or hidden_all % 128 or rows % 16:
        return False
    if (2 * query_first.shape[1]) % 256 or values.shape[2] % 128:
        return False
    cols = -(-hidden_all // (128 * sp)) * 128
    if cols * sp - hidden_all >= cols or cols > hidden_all:
        return False
    if (cols * sp - hidden_all) % 128 or blk % 32:
        return False
    need = 6 * sp * blk * cols + rows * blk * 2 * 20 * sp
    return need < 40 * 1024 * 1024


def one_device(
    axes,
    query_first,
    key_first,
    query_second,
    key_second,
    values,
    lambdas,
    residual,
    norm_gain,
    out_weight,
    gate_weight,
    up_weight,
    down_weight,
):
    if not fits(axes, query_first, values, lambdas, residual, gate_weight):
        return per_device(
            query_first,
            key_first,
            query_second,
            key_second,
            values,
            lambdas,
            residual,
            norm_gain,
            out_weight,
            gate_weight,
            up_weight,
            down_weight,
        )
    n = axes["sp"]
    rows, blk = residual.shape
    hidden_all = gate_weight.shape[1]
    cols = -(-hidden_all // (128 * n)) * 128
    value_size = values.shape[2]
    widths = (query_first.shape[1] // 2, query_second.shape[1] // 2)
    bf16, f32 = jnp.bfloat16, jnp.float32
    vmem = pl.BlockSpec(memory_space=pltpu.VMEM)
    smem = pl.BlockSpec(memory_space=pltpu.SMEM)
    hbm = pl.BlockSpec(memory_space=pl.ANY)
    dma = pltpu.SemaphoreType.DMA
    return pl.pallas_call(
        functools.partial(layer_kernel, n, widths),
        out_shape=jax.ShapeDtypeStruct((rows, blk), bf16),
        in_specs=[vmem] * 5 + [smem, vmem, vmem] + [hbm] * 4,
        out_specs=vmem,
        scratch_shapes=[
            pltpu.VMEM((n,) + key_first.shape, bf16),
            pltpu.VMEM((n,) + key_second.shape, bf16),
            pltpu.VMEM((n,) + values.shape, bf16),
            pltpu.VMEM(out_weight.shape, bf16),
            pltpu.VMEM((4, rows, 1), f32),
            pltpu.VMEM((4, rows, 1), f32),
            pltpu.VMEM((4, rows, value_size), f32),
            pltpu.VMEM((n, blk, cols), bf16),
            pltpu.VMEM((n, blk, cols), bf16),
            pltpu.VMEM((n, cols, blk), bf16),
            pltpu.VMEM((n, rows, blk), bf16),
            pltpu.VMEM((n, rows, blk), bf16),
            pltpu.VMEM((rows, blk), f32),
            pltpu.VMEM((n, n, rows, blk), bf16),
            pltpu.VMEM((n, 16, blk), bf16),
            pltpu.VMEM((n, rows, cols), bf16),
            pltpu.VMEM((n, 2, rows, blk), bf16),
            pltpu.VMEM((n, 2, rows, blk), bf16),
            pltpu.VMEM((n, 2, rows, blk), f32),
            pltpu.VMEM((n, rows, blk), bf16),
            pltpu.VMEM((n, rows, blk), bf16),
            pltpu.VMEM((n, rows, blk), bf16),
            pltpu.VMEM((n, rows, blk), bf16),
            dma((3, n)),
            dma((3, n)),
            dma((3, n)),
            dma((3, n)),
            dma((3, n)),
            dma((3, n)),
            dma((4,)),
            dma((n,)),
            dma((n,)),
            dma((n,)),
            dma((n,)),
            dma((2, n)),
            dma((n,)),
            dma((n,)),
            dma((n,)),
            dma((2, n)),
            dma((2, n)),
            dma((3, n)),
            dma((3, n)),
        ],
        compiler_params=pltpu.CompilerParams(
            collective_id=0, has_side_effects=True, vmem_limit_bytes=60 * 1024 * 1024
        ),
    )(
        query_first,
        query_second,
        key_first,
        key_second,
        values,
        lambdas.T,
        residual,
        norm_gain,
        out_weight,
        gate_weight,
        up_weight,
        down_weight,
    )

def solution(mesh):
    return jax.shard_map(
        functools.partial(one_device, dict(mesh.shape)),
        mesh=mesh,
        in_specs=(
            P(("grp", "sp"), "tp"),
            P(("grp", "sp"), "tp"),
            P(("grp", "sp"), "tp"),
            P(("grp", "sp"), "tp"),
            P(("grp", "sp"), None, "tp"),
            P(None, "tp"),
            P(("grp", "sp"), "tp"),
            P("tp"),
            P(None, "tp", None),
            P("sp", "tp"),
            P("sp", "tp"),
            P("tp", "sp"),
        ),
        out_specs=P(("grp", "sp"), "tp"),
        check_vma=False,
    )
```

profile of v0, /device:TPU:1, one launch (start us, length us, event | category | flops | bytes accessed | tf_op | source)
XLA Modules:
  0.0 120.3 jit_solution(11584496935213578372)
XLA Ops:
  0.0 118.7 %shard_map.118 = bf16[192,512]{1,0:T(8,128)(2,1)} custom-call(bf16[192,128]{1,0:T(8,128)(2,1)} %q1_ref.1, bf16[192,256]{1,0:T(8,128)(2,1)} %q2_ref.1, bf16[192,128]{1,0:T(8,128)(2,1)} %k1_ref.1, bf16[192,256]{1,0:T(8,128)(2,1)} %k2_ref.1, bf16[192,2,128]{2,1,0:T(2,128)(2,1)} %v_ref.1, f32[1,2]{1,0:T(1,128)} %bitcast.1, bf16[192,512]{1,0:T(8,128)(2,1)} %residual_ref.1, ...), custom_call_target="tpu_custom_call" | custom-call | tf_op jit(solution)/shard_map/pallas_call | solution.py:616
  118.7 1.6 %copy.14 = bf16[192,512]{1,0:T(8,128)(2,1)} copy(bf16[192,512]{1,0:T(8,128)(2,1)} %shard_map.118) | data formatting | bytes 393216
where the time goes:
time: 121 us; the launch traced here: 120 us
  Pallas kernels  119 us (98%)
  local copies, waits for them, and re-layouts  1.62 us (1%)
    pallas_call x1, Pallas kernels, one_device(): pl.pallas_call(functools.partial(layer_kernel, n, widths), out_shape=jax....  119 us

commit v1 on v0

--- a/solution.py
+++ b/solution.py
@@ -122,6 +122,102 @@
     return jnp.dot(a, b, preferred_element_type=jnp.float32)
 
 
+def scoped(name):
+    return jax.named_scope(name)
+
+
+PLAN = (
+    {
+        (0, 1): ((1, 0, 3),),
+        (1, 0): ((0, 1, 0),),
+        (1, 1): ((1, 1, 2), (0, 1, 0), (1, 1, 0)),
+        (2, 0): ((1, 2, 0), (0, 2, 0), (0, 2, 1)),
+        (2, 1): ((0, 2, 1), (1, 2, 0), (1, 2, 3), (0, 2, 0)),
+        (3, 0): ((0, 3, 0), (1, 3, 0), (0, 3, 2), (1, 3, 2)),
+        (3, 1): ((0, 3, 0), (0, 3, 2), (0, 3, 1)),
+    },
+    {
+        (0, 0): ((1, 0, 3),),
+        (1, 1): ((0, 1, 2), (2, 2)),
+        (2, 1): ((3, 1),),
+        (3, 1): ((1, 3, 2),),
+    },
+    {
+        (0, 0): ((0, 0, 1),),
+        (1, 0): ((0, 1, 3),),
+        (2, 0): ((0, 3, 0), (0, 1, 3), (0, 2, 3), (1, 3, 0)),
+        (3, 0): ((2, 1),),
+    },
+    {
+        (0, 0): ((0, 0, 3), (1, 0, 1), (2, 1)),
+        (0, 1): ((0, 0, 1),),
+        (1, 0): ((1, 1, 0), (0, 2, 0), (0, 1, 2)),
+        (2, 0): ((1, 2, 1), (2, 1), (3, 3)),
+        (2, 1): ((0, 2, 3), (0, 3, 0), (2, 1)),
+        (3, 0): ((0, 3, 1),),
+    },
+    {
+        (0, 0): ((5, 0), (0, 0, 2), (2, 2), (1, 0, 2), (4, 1), (2, 3), (4, 2)),
+        (0, 1): ((0, 0, 3), (1, 0, 1), (2, 1), (4, 1), (0, 0, 2), (1, 0, 2), (5, 1), (2, 3), (2, 2), (4, 2), (3, 1), (4, 3)),
+        (1, 0): ((2, 2), (1, 1, 3), (0, 0, 3), (2, 0), (0, 3, 0), (4, 0), (1, 0, 3), (1, 3, 0), (1, 1, 2), (5, 2), (5, 0), (3, 2), (0, 0, 2), (4, 2), (4, 3), (1, 2, 0), (1, 0, 2), (2, 3), (3, 3)),
+        (1, 1): ((4, 0), (2, 0), (1, 0, 3), (0, 2, 0), (0, 3, 0), (0, 1, 3), (0, 0, 3), (1, 1, 3), (5, 1), (4, 2), (3, 0), (2, 3), (0, 0, 2), (4, 3), (5, 3), (1, 0, 2)),
+        (2, 0): ((4, 1), (2, 3), (4, 3), (0, 0, 3), (0, 3, 1), (4, 0), (1, 3, 1), (1, 2, 3), (5, 1), (5, 2), (5, 3), (1, 1, 3), (1, 0, 3), (3, 1), (2, 0)),
+        (2, 1): ((0, 3, 1), (4, 1), (2, 3), (4, 0), (0, 1, 3), (4, 3), (1, 3, 1), (0, 0, 3), (1, 1, 3), (1, 3, 0), (1, 2, 1), (1, 0, 3), (5, 0), (2, 0), (3, 0), (5, 3), (5, 1)),
+        (3, 0): ((5, 3), (4, 2), (2, 2), (1, 3, 1), (4, 1), (2, 0), (5, 0), (4, 0), (3, 2)),
+        (3, 1): ((2, 2), (1, 3, 1), (4, 1), (3, 2), (5, 3), (4, 2), (1, 3, 0), (2, 1), (4, 0), (2, 0), (3, 1), (5, 1), (3, 0), (5, 0)),
+    },
+    {
+        (0, 0): ((3, 3), (4, 3), (5, 1), (3, 2), (5, 3), (3, 1), (5, 2)),
+        (0, 1): ((3, 2), (5, 0), (5, 3), (5, 2)),
+        (1, 0): ((3, 0), (5, 3), (5, 1)),
+        (1, 1): ((1, 2, 0), (3, 3), (1, 3, 0), (5, 2), (3, 2)),
+        (2, 0): ((5, 0),),
+        (2, 1): ((5, 2),),
+        (3, 0): ((3, 0), (5, 1), (3, 1)),
+    },
+    {
+        (1, 1): ((5, 0),),
+        (2, 0): ((3, 0),),
+    },
+    {
+        (2, 1): ((3, 3),),
+        (3, 1): ((5, 2),),
+    },
+    {
+        (0, 1): ((3, 3),),
+        (3, 0): ((5, 2),),
+    },
+    {},
+    {},
+    {},
+    {},
+    {},
+    {},
+    {},
+    {},
+    {},
+    {},
+    {},
+    {},
+    {},
+    {},
+    {},
+    {},
+    {},
+    {},
+    {},
+)
+
+WEIGHTS_IN, DOWN_IN, HAND_IN, HAND_DOWN, ROW, ACROSS = range(6)
+
+
+def transit_slot(here, source, target):
+    outer = 0 if source < here else 2
+    if outer:
+        return outer + (target if here == 2 else source - 2)
+    return outer + (target - 2 if here == 1 else source)
+
+
 def layer_kernel(
     sp_count,
     widths,
@@ -148,8 +244,12 @@
     wg,
     wu,
     wd,
+    tg,
+    tu,
+    td,
     mp,
     rsb,
+    mine_ref,
     stream,
     act,
     gains,
@@ -165,6 +265,8 @@
     kv_rs,
     w_ss,
     w_rs,
+    t_ss,
+    t_rs,
     f_ss,
     f_rs,
     own_sem,
@@ -187,9 +289,10 @@
     rows, blk = residual_ref.shape
     cols = wg.shape[2]
     hidden_all = gate_ref.shape[1]
-    value_size = acc.shape[2]
     xpeer, cpeer, dpeer = flip(t, 2), flip(t, 1), flip(t, 3)
     others = range(1, sp_count)
+    everyone = range(sp_count)
+    last = sp_count - 1
 
     def remote(src, dst, ssem, rsem, **where):
         return pltpu.make_async_remote_copy(
@@ -201,86 +304,94 @@
             device_id_type=pl.DeviceIdType.MESH,
         )
 
+    def either(test, action):
+        pl.when(test)(lambda: action(True))
+        pl.when(jnp.logical_not(test))(lambda: action(False))
+
     barrier = pltpu.get_barrier_semaphore()
     for k in others:
         pl.semaphore_signal(barrier, inc=1, device_id={"sp": flip(s, k)}, device_id_type=pl.DeviceIdType.MESH)
         pl.semaphore_signal(barrier, inc=1, device_id={"tp": flip(t, k)}, device_id_type=pl.DeviceIdType.MESH)
     pl.semaphore_signal(barrier, inc=1, device_id={"grp": 1 - y}, device_id_type=pl.DeviceIdType.MESH)
-    pl.semaphore_wait(barrier, 2 * (sp_count - 1) + 1)
+    with scoped("barrier"):
+        pl.semaphore_wait(barrier, 2 * (sp_count - 1) + 1)
 
     sends = []
-
-    right, left = lax.rem(s + 1, sp_count), lax.rem(s + sp_count - 1, sp_count)
-    has_right, has_left = s + 1 < sp_count, s > 0
-
-    def kv_copy(back):
+    half_d = wg.shape[1] // 2
+    extra = sp_count * cols - hidden_all
+    d_half = pl.ds(pl.multiple_of(y * half_d, half_d), half_d)
+
+    def kv_copies(back):
         pairs = ((k1_ref, k1b), (k2_ref, k2b), (v_ref, vb))
+        right = lax.rem(s + 1, sp_count)
         return [
             remote(dst.at[back] if back else src, dst.at[back + 1], kv_ss.at[i, back], kv_rs.at[i, back + 1], sp=right)
             for i, (src, dst) in enumerate(pairs)
         ]
 
-    kv_copies = {back: kv_copy(back) for back in range(sp_count - 1)}
-
-    def kv_send(back):
-        @pl.when(jnp.logical_and(has_right, s >= back))
-        def _():
-            for copy in kv_copies[back]:
-                copy.start()
-
-    kv_send(0)
-
-    half_d = wg.shape[1] // 2
-    half_c = cols // 2
-    extra = sp_count * cols - hidden_all
-    half_last = (cols - extra) // 2
-    d_half = pl.ds(pl.multiple_of(y * half_d, half_d), half_d)
-    last = sp_count - 1
-
-    def w_copy(kind, k, source, target, short):
-        src, dst = ((gate_ref, wg), (up_ref, wu), (down_ref, wd))[kind]
-        begin = hidden_all - cols + extra if short else pl.multiple_of(target * cols, 128)
-        skip, size = (extra, cols - extra) if short else (0, cols)
+    def arrived(back):
+        pairs = ((k1_ref, k1b), (k2_ref, k2b), (v_ref, vb))
+        left = lax.rem(s + sp_count - 1, sp_count)
+        return [
+            remote(src, dst.at[back], kv_ss.at[i, back - 1], kv_rs.at[i, back], sp=left)
+            for i, (src, dst) in enumerate(pairs)
+        ]
+
+    def piece_bounds(target):
+        short = target == last
+        begin = hidden_all - cols + extra if short else target * cols
+        return (begin, extra, cols - extra) if short else (begin, 0, cols)
+
+    def own_piece(kind, target):
+        src = (gate_ref, up_ref, down_ref)[kind]
+        begin, _, size = piece_bounds(target)
         if kind < 2:
-            piece = src.at[d_half, pl.ds(begin, size)]
-            place = dst.at[source, d_half, pl.ds(skip, size)]
+            return src.at[d_half, pl.ds(begin, size)]
+        return src.at[pl.ds(pl.multiple_of(begin + y * (size // 2), 64), size // 2), :]
+
+    def final_place(kind, source, target):
+        dst = (wg, wu, wd)[kind]
+        _, skip, size = piece_bounds(target)
+        if kind < 2:
+            return dst.at[source, d_half, pl.ds(skip, size)]
+        return dst.at[source, pl.ds(pl.multiple_of(skip + y * (size // 2), 64), size // 2)]
+
+    def transit_place(kind, here, source, target):
+        buffer = (tg, tu, td)[kind].at[transit_slot(here, source, target)]
+        _, _, size = piece_bounds(target)
+        return buffer.at[:, pl.ds(0, size)] if kind < 2 else buffer.at[pl.ds(0, size // 2)]
+
+    def weight_hop(kind, here, source, target):
+        there = here + 1 if target > here else here - 1
+        if source == here:
+            piece, ssem = own_piece(kind, target), w_ss.at[kind, target]
         else:
-            part = y * (size // 2)
-            piece = src.at[pl.ds(pl.multiple_of(begin + part, 64), size // 2), :]
-            place = dst.at[source, pl.ds(pl.multiple_of(skip + part, 64), size // 2)]
-        return remote(piece, place, w_ss.at[kind, k], w_rs.at[kind, k], sp=flip(s, k)), place
-
-    def f_copy(kind, k, short):
-        _, place = w_copy(kind, k, flip(s, k), s, short)
-        return remote(place, place, f_ss.at[kind, k], f_rs.at[kind, k], grp=1 - y)
-
-    def either(test, action):
-        pl.when(test)(lambda: action(True))
-        pl.when(jnp.logical_not(test))(lambda: action(False))
-
-    def send_weights(kinds, rightward):
-        for k in others:
-
-            def go(short, k=k):
-                for kind in kinds:
-                    w_copy(kind, k, s, flip(s, k), short)[0].start()
-
-            target = flip(s, k)
-            if rightward:
-                pl.when(target == last)(functools.partial(go, True))
-                pl.when(jnp.logical_and(target > s, target != last))(functools.partial(go, False))
-            else:
-                pl.when(target < s)(functools.partial(go, False))
-
-    @pl.when(s == last)
-    def _():
-        wg[:, :, :extra] = jnp.zeros((sp_count, wg.shape[1], extra), jnp.bfloat16)
-        wu[:, :, :extra] = jnp.zeros((sp_count, wg.shape[1], extra), jnp.bfloat16)
-        wd[:, :extra, :] = jnp.zeros((sp_count, extra, blk), jnp.bfloat16)
-
-    send_weights((0, 1), False)
-    proj_copy = pltpu.make_async_copy(proj_hbm, proj_ref, own_sem.at[3])
-    proj_copy.start()
+            piece, ssem = transit_place(kind, here, source, target), t_ss.at[kind, transit_slot(here, source, target)]
+        if there == target:
+            place, rsem = final_place(kind, source, target), w_rs.at[kind, source]
+        else:
+            place, rsem = transit_place(kind, there, source, target), t_rs.at[kind, transit_slot(there, source, target)]
+        return remote(piece, place, ssem, rsem, sp=there)
+
+    def move_weights(kinds, here, source, target):
+        for kind in kinds:
+            if source != here:
+                before = here - 1 if source < here else here + 1
+                with scoped(f"pass{kind}_{source}{target}"):
+                    weight_hop(kind, before, source, target).wait_recv()
+            weight_hop(kind, here, source, target).start()
+
+    def weight_hand(kind, source, target):
+        place = final_place(kind, source, target)
+        return remote(place, place, f_ss.at[kind, source], f_rs.at[kind, source], grp=1 - y)
+
+    def hand_over(kinds, here, source):
+        for kind in kinds:
+            before = here - 1 if source < here else here + 1
+            with scoped(f"hand{kind}_{source}"):
+                weight_hop(kind, before, source, here).wait_recv()
+            weight_hand(kind, source, here).start()
+
     def own_copy(kind, short):
         src, dst = ((gate_ref, wg), (up_ref, wu), (down_ref, wd))[kind]
         begin = hidden_all - cols + extra if short else pl.multiple_of(s * cols, 128)
@@ -288,6 +399,85 @@
         if kind < 2:
             return pltpu.make_async_copy(src.at[:, pl.ds(begin, size)], dst.at[s, :, pl.ds(skip, size)], own_sem.at[kind])
         return pltpu.make_async_copy(src.at[pl.ds(begin, size), :], dst.at[s, pl.ds(skip, size)], own_sem.at[kind])
+
+    def act_z(row, begin, target, way):
+        piece = act.at[t, row]
+        return remote(piece, piece, az_ss.at[way, row], az_rs.at[row], sp=target)
+
+    def along(here, row, action):
+        if row <= here < last:
+            action(act_z(row, here, here + 1, 0))
+        if row >= here > 0:
+            action(act_z(row, here, here - 1, 1))
+
+    def act_x(row):
+        piece = act.at[t, row]
+        return remote(piece, piece, ax_ss.at[row], ax_rs.at[row], tp=xpeer)
+
+    def act_c(row, second):
+        piece = act.at[xpeer if second else t, row]
+        return remote(piece, piece, ac_ss.at[second, row], ac_rs.at[second, row], tp=cpeer)
+
+    def start(copy):
+        copy.start()
+
+    def perform(here, event):
+        kind, index = event[:2]
+        if kind == WEIGHTS_IN:
+            move_weights((0, 1), here, index, event[2])
+        elif kind == DOWN_IN:
+            move_weights((2,), here, index, event[2])
+        elif kind == HAND_IN:
+            hand_over((0, 1), here, index)
+        elif kind == HAND_DOWN:
+            hand_over((2,), here, index)
+        elif kind == ROW:
+            with scoped(f"row{index}"):
+                act_z(index, here, here, 0).wait_recv()
+            send_row(here, index)
+        elif kind == ACROSS:
+            with scoped(f"across{index}"):
+                act_x(index).wait_recv()
+            act_c(index, 1).start()
+
+    def send_row(here, row):
+        along(here, row, start)
+        act_x(row).start()
+        act_c(row, 0).start()
+
+    x = t // 2
+    steps = iter(PLAN)
+
+    def next_step():
+        plan = next(steps)
+        for here in everyone:
+            lists = [plan.get((here, side), ()) for side in range(2)]
+            tests = [(s == here, lists[0])]
+            if lists[0] != lists[1]:
+                tests = [(jnp.logical_and(s == here, x == side), lists[side]) for side in range(2)]
+            for test, events in tests:
+                if events:
+
+                    @pl.when(test)
+                    def _(here=here, events=events):
+                        for event in events:
+                            perform(here, event)
+
+    next_step()
+
+    @pl.when(s < last)
+    def _():
+        for copy in kv_copies(0):
+            copy.start()
+
+    @pl.when(s == last)
+    def _():
+        wg[:, :, :extra] = jnp.zeros((sp_count, wg.shape[1], extra), jnp.bfloat16)
+        wu[:, :, :extra] = jnp.zeros((sp_count, wg.shape[1], extra), jnp.bfloat16)
+        wd[:, :extra, :] = jnp.zeros((sp_count, extra, blk), jnp.bfloat16)
+
+    proj_copy = pltpu.make_async_copy(proj_hbm, proj_ref, own_sem.at[3])
+    proj_copy.start()
 
     def start_own(short):
         for kind in range(3):
@@ -339,218 +529,228 @@
                     total[state] = total[state] * fade + jnp.sum(weights, axis=1, keepdims=True)
                     acc[state] = acc[state] * fade + dot(weights.astype(jnp.bfloat16), values)
 
-    block((k1_ref, k2_ref), v_ref, True)
+    with scoped("diag"):
+        block((k1_ref, k2_ref), v_ref, True)
     for back in others:
 
         @pl.when(s >= back)
         def _(back=back):
-            for copy in kv_copies[back - 1]:
-                copy.wait_recv()
-
-        if back in kv_copies:
-            kv_send(back)
-        if back == sp_count - 2:
-            send_weights((0, 1), True)
-
-        @pl.when(s >= back)
-        def _(back=back):
-            block((k1b.at[back], k2b.at[back]), vb.at[back], False)
-
+            with scoped(f"kvwait{back}"):
+                for i, copy in enumerate(arrived(back)):
+                    copy.wait_recv()
+                    if back < last:
+                        pl.when(s < last)(kv_copies(back)[i].start)
+            with scoped(f"block{back}"):
+                block((k1b.at[back], k2b.at[back]), vb.at[back], False)
+
+    next_step()
     proj_copy.wait()
-    attended = []
-    for group in range(2):
-        first = acc[2 * group] / total[2 * group]
-        second = acc[2 * group + 1] / total[2 * group + 1]
-        differ = first - lam_ref[0, group] * second
-        scale = lax.rsqrt(jnp.mean(differ * differ, axis=1, keepdims=True) + 1e-06)
-        attended.append((0.8 * differ * scale).astype(jnp.bfloat16))
+    with scoped("finish"):
+        attended = []
+        for group in range(2):
+            first = acc[2 * group] / total[2 * group]
+            second = acc[2 * group + 1] / total[2 * group + 1]
+            differ = first - lam_ref[0, group] * second
+            scale = lax.rsqrt(jnp.mean(differ * differ, axis=1, keepdims=True) + 1e-06)
+            attended.append((0.8 * differ * scale).astype(jnp.bfloat16))
 
     def project(owner):
         columns = pl.ds(pl.multiple_of(owner * blk, blk), blk)
         return dot(attended[0], proj_ref[0, :, columns]) + dot(attended[1], proj_ref[1, :, columns])
 
-    def hand_over(kinds, k):
+    with scoped("project"):
+        mp[0] = project(cpeer).astype(jnp.bfloat16)
+        mp[1] = project(dpeer).astype(jnp.bfloat16)
+        to_core = remote(mp.at[pl.ds(0, 2)], rsb.at[pl.ds(0, 2)], rs_ss.at[0], rs_rs.at[0], tp=cpeer)
+        to_core.start()
+        to_x = remote(mp.at[2], rsb.at[2], rs_ss.at[1], rs_rs.at[1], tp=xpeer)
+        sends.extend((to_core, to_x))
+        mine_ref[1] = project(xpeer)
+        mine_ref[0] = residual_ref[...].astype(jnp.float32) + project(t)
+    next_step()
+    with scoped("rscore"):
+        to_core.wait_recv()
+    mp[2] = (mine_ref[1] + rsb[1].astype(jnp.float32)).astype(jnp.bfloat16)
+    to_x.start()
+    mine_ref[0] = mine_ref[0] + rsb[0].astype(jnp.float32)
+    next_step()
+    with scoped("rsx"):
+        to_x.wait_recv()
+    stream[...] = mine_ref[0] + rsb[2].astype(jnp.float32)
+    act[t, s] = stream[...].astype(jnp.bfloat16)
+
+    for here in everyone:
+
+        @pl.when(s == here)
+        def _(here=here):
+            send_row(here, here)
+
+    next_step()
+
+    for copy in gain_copies:
+        copy.wait_recv()
+
+    def place_of(kind, source, short):
+        size = cols - extra if short else cols
+        skip = extra if short else 0
+        if kind < 2:
+            half = pl.ds(pl.multiple_of((1 - y) * half_d, half_d), half_d)
+            return (wg, wu)[kind].at[source, half, pl.ds(skip, size)]
+        part = (1 - y) * (size // 2)
+        return wd.at[source, pl.ds(pl.multiple_of(skip + part, 64), size // 2)]
+
+    def await_weights(kinds, source):
         def go(short):
             for kind in kinds:
-                w_copy(kind, k, flip(s, k), s, short)[0].wait_recv()
-                f_copy(kind, k, short).start()
+                place = place_of(kind, source, short)
+
+                @pl.when(source != s)
+                def _(kind=kind, place=place):
+                    remote(place, place, f_ss.at[kind, source], f_rs.at[kind, source], grp=1 - y).wait_recv()
+
+                @pl.when(source == s)
+                def _(kind=kind):
+                    own_copy(kind, short).wait()
 
         either(s == last, go)
 
-    rs_copies = {}
-    for k in (2, 3, 1):
-        mp[k] = project(flip(t, k)).astype(jnp.bfloat16)
-        rs_copies[k] = remote(mp.at[k], rsb.at[k], rs_ss.at[k], rs_rs.at[k], tp=flip(t, k))
-        rs_copies[k].start()
-        sends.append(rs_copies[k])
-    mixed = project(t)
-    hand_over((0, 1), 1)
-    for k in (1, 2, 3):
-        rs_copies[k].wait_recv()
-        mixed = mixed + rsb[k].astype(jnp.float32)
-    stream[...] = residual_ref[...].astype(jnp.float32) + mixed
-    act[t, s] = stream[...].astype(jnp.bfloat16)
-
-    ax, ac0, ac1 = {}, {}, {}
-    for k in range(sp_count):
-        row = flip(s, k)
-        ax[k] = remote(act.at[t, row], act.at[t, row], ax_ss.at[k], ax_rs.at[k], tp=xpeer)
-        ac0[k] = remote(act.at[t, row], act.at[t, row], ac_ss.at[0, k], ac_rs.at[0, k], tp=cpeer)
-        ac1[k] = remote(act.at[xpeer, row], act.at[xpeer, row], ac_ss.at[1, k], ac_rs.at[1, k], tp=cpeer)
-
-    def along_line(k, action):
-        row = flip(s, k)
-        piece = act.at[t, row]
-
-        @pl.when(jnp.logical_and(has_right, row <= s))
-        def _():
-            action(remote(piece, piece, az_ss.at[0, row], az_rs.at[row], sp=right))
-
-        @pl.when(jnp.logical_and(has_left, row >= s))
-        def _():
-            action(remote(piece, piece, az_ss.at[1, row], az_rs.at[row], sp=left))
-
-    along_line(0, lambda copy: copy.start())
-    send_weights((2,), True)
-    send_weights((2,), False)
-
-    def pass_on(k):
-        if k:
-            row = flip(s, k)
-            piece = act.at[t, row]
-            remote(piece, piece, az_ss.at[0, row], az_rs.at[row], sp=right).wait_recv()
-            along_line(k, lambda copy: copy.start())
-        ax[k].start()
-        ac0[k].start()
-
-    def pass_inside(k):
-        ax[k].wait_recv()
-        ac1[k].start()
-
-    def await_weights(kinds):
-        def go(short):
-            for kind in kinds:
-                own_copy(kind, short).wait()
-                for k in others:
-                    f_copy(kind, k, short).wait_recv()
-
-        either(s == last, go)
-
-    turns = (0, 1, 3, 2)
-    pass_on(0)
-    for at, k in enumerate(turns[1:]):
-        if at + 2 < sp_count:
-            hand_over((0, 1), at + 2)
-        pass_on(k)
-        pass_inside(turns[at])
-    pass_inside(turns[-1])
-
-    for copy in gain_copies:
-        copy.wait_recv()
-    await_weights((0, 1))
+    with scoped("await_gu"):
+        for source in everyone:
+            await_weights((0, 1), source)
     column = jnp.minimum(s * cols, hidden_all - cols) + lax.broadcasted_iota(jnp.int32, (1, cols), 1)
     mine = column >= s * cols
 
     def hidden_of(k):
         row = flip(s, k)
-        ac0[k].wait_recv()
-        ac1[k].wait_recv()
-        squares = jnp.zeros((rows, 1), jnp.float32)
-        for part in range(sp_count):
-            piece = act[part, row].astype(jnp.float32)
-            squares = squares + jnp.sum(piece * piece, axis=1, keepdims=True)
-        scale = lax.rsqrt(squares / (sp_count * blk) + 1e-06)
-        gate = jnp.zeros((rows, cols), jnp.float32)
-        up = jnp.zeros((rows, cols), jnp.float32)
-        for part in range(sp_count):
-            gain = gains[part, 0:1, :].astype(jnp.float32)
-            normed = (act[part, row].astype(jnp.float32) * scale * gain).astype(jnp.bfloat16)
-            gate = gate + dot(normed, wg[part])
-            up = up + dot(normed, wu[part])
-        hidden = gate / (1.0 + jnp.exp(-gate)) * up
-        hid[k] = jnp.where(mine, hidden, 0.0).astype(jnp.bfloat16)
-
-    r1, r2, r3 = {}, {}, {}
-    for k in range(sp_count):
-        r1[k] = remote(c1.at[k], c1r.at[k], c_ss.at[0, k], c_rs.at[0, k], tp=cpeer)
+        next_step()
+        with scoped(f"acwait{k}"):
+            act_c(row, 0).wait_recv()
+            act_c(row, 1).wait_recv()
+        with scoped(f"hidden{k}"):
+            squares = jnp.zeros((rows, 1), jnp.float32)
+            for part in range(sp_count):
+                piece = act[part, row].astype(jnp.float32)
+                squares = squares + jnp.sum(piece * piece, axis=1, keepdims=True)
+            scale = lax.rsqrt(squares / (sp_count * blk) + 1e-06)
+            gate = jnp.zeros((rows, cols), jnp.float32)
+            up = jnp.zeros((rows, cols), jnp.float32)
+            for part in range(sp_count):
+                gain = gains[part, 0:1, :].astype(jnp.float32)
+                normed = (act[part, row].astype(jnp.float32) * scale * gain).astype(jnp.bfloat16)
+                gate = gate + dot(normed, wg[part])
+                up = up + dot(normed, wu[part])
+            hidden = gate / (1.0 + jnp.exp(-gate)) * up
+            hid[k] = jnp.where(mine, hidden, 0.0).astype(jnp.bfloat16)
+
+    r1a, r1b, r2 = {}, {}, {}
+    for k in everyone:
+        r1a[k] = remote(c1.at[k, 1], c1r.at[k, 1], c_ss.at[0, k], c_rs.at[0, k], tp=cpeer)
+        r1b[k] = remote(c1.at[k, 0], c1r.at[k, 0], c_ss.at[3, k], c_rs.at[3, k], tp=cpeer)
         r2[k] = remote(c2.at[k], c2r.at[k], c_ss.at[1, k], c_rs.at[1, k], tp=xpeer)
-        if k:
-            r3[k] = remote(c3.at[k], c3r.at[k], c_ss.at[2, k], c_rs.at[2, k], sp=flip(s, k))
-
-    def down_of(k):
-        hidden = hid[k]
-        c1[k, 0] = dot(hidden, wd[cpeer]).astype(jnp.bfloat16)
-        c1[k, 1] = dot(hidden, wd[dpeer]).astype(jnp.bfloat16)
-        r1[k].start()
-        po[k, 1] = dot(hidden, wd[xpeer])
-        po[k, 0] = dot(hidden, wd[t])
-
-    def across(k):
-        r1[k].wait_recv()
+    r3 = {k: remote(c3.at[k], c3r.at[k], c_ss.at[2, k], c_rs.at[2, k], sp=flip(s, k - 2 if k == 3 else k)) for k in others}
+
+    def cross(k):
+        next_step()
+        with scoped(f"cross{k}"):
+            c1[k, 1] = dot(hid[k], wd[dpeer]).astype(jnp.bfloat16)
+            r1a[k].start()
+            po[k, 1] = dot(hid[k], wd[xpeer])
+
+    def to_other_chip(k):
+        next_step()
+        with scoped(f"r1a{k}"):
+            r1a[k].wait_recv()
         c2[k] = (po[k, 1] + c1r[k, 1].astype(jnp.float32)).astype(jnp.bfloat16)
         r2[k].start()
 
-    def along(k):
-        r2[k].wait_recv()
+    def near(k):
+        next_step()
+        with scoped(f"near{k}"):
+            c1[k, 0] = dot(hid[k], wd[cpeer]).astype(jnp.bfloat16)
+            r1b[k].start()
+            po[k, 0] = dot(hid[k], wd[t])
+
+    def finish_row(k):
+        next_step()
+        with scoped(f"r1b{k}"):
+            r1b[k].wait_recv()
+        with scoped(f"r2_{k}"):
+            r2[k].wait_recv()
         result = po[k, 0] + c1r[k, 0].astype(jnp.float32) + c2r[k].astype(jnp.float32)
+        if k == 2:
+            with scoped("r3_3"):
+                r3[3].wait_recv()
+            result = result + c3r[3].astype(jnp.float32)
         if k:
             c3[k] = result.astype(jnp.bfloat16)
             r3[k].start()
         else:
             po[0, 0] = result
 
-    for at, k in enumerate(turns):
-        hidden_of(k)
-        if at + 1 < sp_count:
-            hand_over((2,), at + 1)
-    await_weights((2,))
-    order = (3, 2, 1, 0)
-    for at, k in enumerate(order):
-        down_of(k)
-        if at >= 1:
-            across(order[at - 1])
-        if at >= 2:
-            along(order[at - 2])
-    across(order[-1])
-    along(order[-2])
-    along(order[-1])
-
+    hidden_of(3)
+    next_step()
+    with scoped("await_cross"):
+        await_weights((2,), dpeer)
+        await_weights((2,), xpeer)
+    cross(3)
+    hidden_of(2)
+    to_other_chip(3)
+    cross(2)
+    hidden_of(1)
+    to_other_chip(2)
+    cross(1)
+    hidden_of(0)
+    to_other_chip(1)
+    cross(0)
+    to_other_chip(0)
+    next_step()
+    with scoped("await_near"):
+        await_weights((2,), cpeer)
+        await_weights((2,), t)
+    near(3)
+    near(2)
+    finish_row(3)
+    near(1)
+    near(0)
+    finish_row(2)
+    finish_row(1)
+    finish_row(0)
+
+    next_step()
     ffn = po[0, 0]
-    for k in order[:-1]:
-        r3[k].wait_recv()
+    for k in (1, 2):
+        with scoped(f"r3_{k}"):
+            r3[k].wait_recv()
         ffn = ffn + c3r[k].astype(jnp.float32)
     out_ref[...] = (stream[...] + 0.5 * ffn).astype(jnp.bfloat16)
 
-    for back in kv_copies:
-
-        @pl.when(jnp.logical_and(has_right, s >= back))
-        def _(back=back):
-            for copy in kv_copies[back]:
-                copy.wait_send()
-
-    def finish():
-        for k in others:
-
-            def go(short, k=k):
+    with scoped("drain"):
+        for here in everyone:
+
+            @pl.when(s == here)
+            def _(here=here):
+                if here < last:
+                    for back in range(here + 1):
+                        for copy in kv_copies(back):
+                            copy.wait_send()
                 for kind in range(3):
-                    w_copy(kind, k, s, flip(s, k), short)[0].wait_send()
-
-            either(flip(s, k) == last, go)
-
-        def gone(short):
-            for k in others:
-                for kind in range(3):
-                    f_copy(kind, k, short).wait_send()
-
-        either(s == last, gone)
-
-    finish()
-    for k in range(sp_count):
-        along_line(k, lambda copy: copy.wait_send())
-    for copies in (ax, ac0, ac1, r1, r2, r3):
-        sends.extend(copies.values())
-    for copy in sends:
-        copy.wait_send()
+                    for there in everyone:
+                        if there != here:
+                            weight_hop(kind, here, here, there).wait_send()
+                            weight_hand(kind, there, here).wait_send()
+                    for source in everyone:
+                        for target in everyone:
+                            if min(source, target) < here < max(source, target):
+                                weight_hop(kind, here, source, target).wait_send()
+                for row in everyone:
+                    along(here, row, lambda copy: copy.wait_send())
+
+        for row in everyone:
+            sends.extend((act_x(row), act_c(row, 0), act_c(row, 1)))
+        for copies in (r1a, r1b, r2, r3):
+            sends.extend(copies.values())
+        for copy in sends:
+            copy.wait_send()
 
 
 def fits(axes, query_first, values, lambdas, residual, gate_weight):
@@ -629,8 +829,12 @@
             pltpu.VMEM((n, blk, cols), bf16),
             pltpu.VMEM((n, blk, cols), bf16),
             pltpu.VMEM((n, cols, blk), bf16),
-            pltpu.VMEM((n, rows, blk), bf16),
-            pltpu.VMEM((n, rows, blk), bf16),
+            pltpu.VMEM((4, blk // 2, cols), bf16),
+            pltpu.VMEM((4, blk // 2, cols), bf16),
+            pltpu.VMEM((4, cols // 2, blk), bf16),
+            pltpu.VMEM((3, rows, blk), bf16),
+            pltpu.VMEM((3, rows, blk), bf16),
+            pltpu.VMEM((2, rows, blk), f32),
             pltpu.VMEM((rows, blk), f32),
             pltpu.VMEM((n, n, rows, blk), bf16),
             pltpu.VMEM((n, 16, blk), bf16),
@@ -648,19 +852,21 @@
             dma((3, n)),
             dma((3, n)),
             dma((3, n)),
+            dma((3, n)),
+            dma((3, n)),
             dma((4,)),
             dma((n,)),
             dma((n,)),
-            dma((n,)),
-            dma((n,)),
+            dma((2,)),
+            dma((2,)),
             dma((2, n)),
             dma((n,)),
             dma((n,)),
             dma((n,)),
             dma((2, n)),
             dma((2, n)),
-            dma((3, n)),
-            dma((3, n)),
+            dma((4, n)),
+            dma((4, n)),
         ],
         compiler_params=pltpu.CompilerParams(
             collective_id=0, has_side_effects=True, vmem_limit_bytes=60 * 1024 * 1024

time: 121 us -> 102 us (0.84)
  the two profiles are of different devices: /device:TPU:1 before, /device:TPU:18 now
where the time goes in v1:
time: 102 us
  Pallas kernels  101 us (99%)
  local copies, waits for them, and re-layouts  1.62 us (2%)
    pallas_call x1, Pallas kernels, one_device(): pl.pallas_call(functools.partial(layer_kernel, n, widths), out_shape=jax....  101 us

profile of v1, /device:TPU:18, one launch (start us, length us, event | category | flops | bytes accessed | tf_op | source)
XLA Modules:
  0.0 102.2 jit_solution(17725955004334865740)
XLA Ops:
  0.0 100.5 %shard_map.118 = bf16[192,512]{1,0:T(8,128)(2,1)} custom-call(bf16[192,128]{1,0:T(8,128)(2,1)} %q1_ref.1, bf16[192,256]{1,0:T(8,128)(2,1)} %q2_ref.1, bf16[192,128]{1,0:T(8,128)(2,1)} %k1_ref.1, bf16[192,256]{1,0:T(8,128)(2,1)} %k2_ref.1, bf16[192,2,128]{2,1,0:T(2,128)(2,1)} %v_ref.1, f32[1,2]{1,0:T(1,128)} %bitcast.1, bf16[192,512]{1,0:T(8,128)(2,1)} %residual_ref.1, ...), custom_call_target="tpu_custom_call" | custom-call | tf_op jit(solution)/shard_map/pallas_call | solution.py:816
  100.5 1.6 %copy.14 = bf16[192,512]{1,0:T(8,128)(2,1)} copy(bf16[192,512]{1,0:T(8,128)(2,1)} %shard_map.118) | data formatting | bytes 393216

commit v2 on v1

--- a/solution.py
+++ b/solution.py
@@ -128,65 +128,61 @@
 
 PLAN = (
     {
-        (0, 1): ((1, 0, 3),),
         (1, 0): ((0, 1, 0),),
-        (1, 1): ((1, 1, 2), (0, 1, 0), (1, 1, 0)),
-        (2, 0): ((1, 2, 0), (0, 2, 0), (0, 2, 1)),
-        (2, 1): ((0, 2, 1), (1, 2, 0), (1, 2, 3), (0, 2, 0)),
-        (3, 0): ((0, 3, 0), (1, 3, 0), (0, 3, 2), (1, 3, 2)),
-        (3, 1): ((0, 3, 0), (0, 3, 2), (0, 3, 1)),
+        (1, 1): ((1, 1, 3), (0, 1, 0)),
+        (2, 0): ((0, 2, 0), (1, 2, 1), (1, 2, 3), (1, 2, 0)),
+        (2, 1): ((0, 2, 3), (1, 2, 1), (0, 2, 0), (1, 2, 0)),
+        (3, 0): ((1, 3, 0), (0, 3, 0), (0, 3, 1), (0, 3, 2), (1, 3, 2)),
+        (3, 1): ((0, 3, 0), (1, 3, 0), (0, 3, 2), (1, 3, 1)),
+    },
+    {
+        (0, 0): ((0, 0, 2),),
+        (0, 1): ((0, 0, 1),),
+        (1, 0): ((0, 1, 3),),
+        (2, 0): ((0, 2, 1),),
+        (2, 1): ((0, 3, 0), (1, 1, 3)),
+    },
+    {
+        (1, 1): ((0, 1, 2), (0, 2, 0)),
+        (2, 0): ((1, 3, 0),),
+        (2, 1): ((0, 2, 1), (2, 3)),
+        (3, 1): ((0, 3, 1),),
     },
     {
         (0, 0): ((1, 0, 3),),
-        (1, 1): ((0, 1, 2), (2, 2)),
-        (2, 1): ((3, 1),),
-        (3, 1): ((1, 3, 2),),
+        (0, 1): ((2, 1),),
+        (1, 0): ((0, 1, 2), (0, 2, 0)),
+        (1, 1): ((1, 2, 0), (3, 2), (0, 1, 3)),
+        (2, 0): ((0, 1, 3), (0, 2, 3), (0, 3, 0), (2, 3)),
     },
     {
-        (0, 0): ((0, 0, 1),),
-        (1, 0): ((0, 1, 3),),
-        (2, 0): ((0, 3, 0), (0, 1, 3), (0, 2, 3), (1, 3, 0)),
-        (3, 0): ((2, 1),),
+        (0, 0): ((2, 1), (0, 0, 3), (2, 2), (4, 1), (0, 0, 1), (3, 3), (1, 0, 2), (5, 1), (1, 0, 1), (2, 3), (4, 2), (4, 3), (3, 2), (5, 0), (3, 1), (5, 2), (5, 3)),
+        (0, 1): ((0, 0, 2), (5, 0), (1, 0, 3), (1, 0, 1), (4, 1), (5, 1), (0, 0, 3), (2, 2), (1, 0, 2), (3, 2), (3, 1), (2, 3), (3, 3), (4, 2), (4, 3), (5, 2), (5, 3)),
+        (1, 0): ((4, 0), (1, 1, 0), (0, 0, 3), (3, 2), (1, 3, 0), (0, 0, 2), (2, 2), (1, 0, 3), (0, 3, 0), (2, 0), (4, 2), (4, 3), (1, 0, 2), (1, 2, 0), (1, 1, 3), (1, 1, 2), (2, 3), (5, 1), (3, 3), (3, 0), (5, 2), (5, 3), (5, 0)),
+        (1, 1): ((4, 0), (1, 1, 0), (0, 0, 2), (2, 0), (0, 3, 0), (5, 1), (1, 1, 2), (4, 2), (2, 2), (0, 0, 3), (3, 0), (1, 3, 0), (4, 3), (5, 0), (1, 0, 3), (1, 0, 2), (2, 3), (5, 2), (3, 3), (5, 3)),
+        (2, 0): ((2, 1), (4, 0), (4, 3), (5, 0), (0, 0, 3), (3, 3), (0, 3, 1), (5, 2), (4, 1), (2, 0), (1, 3, 1), (5, 3), (3, 0), (1, 0, 3), (5, 1)),
+        (2, 1): ((1, 3, 0), (4, 1), (2, 1), (4, 0), (4, 3), (1, 2, 3), (2, 0), (0, 3, 1), (0, 1, 3), (1, 3, 1), (5, 0), (3, 3), (3, 1), (5, 2), (5, 3), (0, 0, 3)),
+        (3, 0): ((1, 3, 1), (2, 2), (3, 2), (4, 2), (4, 0), (2, 1), (2, 0), (4, 1), (5, 0), (3, 0)),
+        (3, 1): ((1, 3, 2), (4, 2), (3, 1), (2, 2), (4, 0), (4, 1), (3, 2), (2, 1), (5, 0), (5, 2), (2, 0), (3, 0), (5, 3), (5, 1)),
     },
     {
-        (0, 0): ((0, 0, 3), (1, 0, 1), (2, 1)),
-        (0, 1): ((0, 0, 1),),
-        (1, 0): ((1, 1, 0), (0, 2, 0), (0, 1, 2)),
-        (2, 0): ((1, 2, 1), (2, 1), (3, 3)),
-        (2, 1): ((0, 2, 3), (0, 3, 0), (2, 1)),
-        (3, 0): ((0, 3, 1),),
+        (2, 1): ((1, 0, 3), (5, 1), (3, 0)),
     },
     {
-        (0, 0): ((5, 0), (0, 0, 2), (2, 2), (1, 0, 2), (4, 1), (2, 3), (4, 2)),
-        (0, 1): ((0, 0, 3), (1, 0, 1), (2, 1), (4, 1), (0, 0, 2), (1, 0, 2), (5, 1), (2, 3), (2, 2), (4, 2), (3, 1), (4, 3)),
-        (1, 0): ((2, 2), (1, 1, 3), (0, 0, 3), (2, 0), (0, 3, 0), (4, 0), (1, 0, 3), (1, 3, 0), (1, 1, 2), (5, 2), (5, 0), (3, 2), (0, 0, 2), (4, 2), (4, 3), (1, 2, 0), (1, 0, 2), (2, 3), (3, 3)),
-        (1, 1): ((4, 0), (2, 0), (1, 0, 3), (0, 2, 0), (0, 3, 0), (0, 1, 3), (0, 0, 3), (1, 1, 3), (5, 1), (4, 2), (3, 0), (2, 3), (0, 0, 2), (4, 3), (5, 3), (1, 0, 2)),
-        (2, 0): ((4, 1), (2, 3), (4, 3), (0, 0, 3), (0, 3, 1), (4, 0), (1, 3, 1), (1, 2, 3), (5, 1), (5, 2), (5, 3), (1, 1, 3), (1, 0, 3), (3, 1), (2, 0)),
-        (2, 1): ((0, 3, 1), (4, 1), (2, 3), (4, 0), (0, 1, 3), (4, 3), (1, 3, 1), (0, 0, 3), (1, 1, 3), (1, 3, 0), (1, 2, 1), (1, 0, 3), (5, 0), (2, 0), (3, 0), (5, 3), (5, 1)),
-        (3, 0): ((5, 3), (4, 2), (2, 2), (1, 3, 1), (4, 1), (2, 0), (5, 0), (4, 0), (3, 2)),
-        (3, 1): ((2, 2), (1, 3, 1), (4, 1), (3, 2), (5, 3), (4, 2), (1, 3, 0), (2, 1), (4, 0), (2, 0), (3, 1), (5, 1), (3, 0), (5, 0)),
+        (3, 0): ((5, 1), (3, 1)),
     },
     {
-        (0, 0): ((3, 3), (4, 3), (5, 1), (3, 2), (5, 3), (3, 1), (5, 2)),
-        (0, 1): ((3, 2), (5, 0), (5, 3), (5, 2)),
-        (1, 0): ((3, 0), (5, 3), (5, 1)),
-        (1, 1): ((1, 2, 0), (3, 3), (1, 3, 0), (5, 2), (3, 2)),
-        (2, 0): ((5, 0),),
-        (2, 1): ((5, 2),),
-        (3, 0): ((3, 0), (5, 1), (3, 1)),
+        (3, 0): ((5, 3), (5, 2)),
     },
     {
-        (1, 1): ((5, 0),),
-        (2, 0): ((3, 0),),
+        (2, 0): ((1, 1, 3),),
     },
+    {},
+    {},
+    {},
     {
-        (2, 1): ((3, 3),),
-        (3, 1): ((5, 2),),
+        (2, 0): ((3, 1),),
     },
-    {
-        (0, 1): ((3, 3),),
-        (3, 0): ((5, 2),),
-    },
     {},
     {},
     {},
@@ -209,6 +205,9 @@
 )
 
 WEIGHTS_IN, DOWN_IN, HAND_IN, HAND_DOWN, ROW, ACROSS = range(6)
+
+
+PARTS = 2
 
 
 def transit_slot(here, source, target):
@@ -316,7 +315,6 @@
     with scoped("barrier"):
         pl.semaphore_wait(barrier, 2 * (sp_count - 1) + 1)
 
-    sends = []
     half_d = wg.shape[1] // 2
     extra = sp_count * cols - hidden_all
     d_half = pl.ds(pl.multiple_of(y * half_d, half_d), half_d)
@@ -325,7 +323,7 @@
         pairs = ((k1_ref, k1b), (k2_ref, k2b), (v_ref, vb))
         right = lax.rem(s + 1, sp_count)
         return [
-            remote(dst.at[back] if back else src, dst.at[back + 1], kv_ss.at[i, back], kv_rs.at[i, back + 1], sp=right)
+            remote(dst.at[back] if back else src, dst.at[back + 1], kv_ss.at[i], kv_rs.at[i, back], sp=right)
             for i, (src, dst) in enumerate(pairs)
         ]
 
@@ -333,7 +331,7 @@
         pairs = ((k1_ref, k1b), (k2_ref, k2b), (v_ref, vb))
         left = lax.rem(s + sp_count - 1, sp_count)
         return [
-            remote(src, dst.at[back], kv_ss.at[i, back - 1], kv_rs.at[i, back], sp=left)
+            remote(src, dst.at[back], kv_ss.at[i], kv_rs.at[i, back - 1], sp=left)
             for i, (src, dst) in enumerate(pairs)
         ]
 
@@ -342,55 +340,68 @@
         begin = hidden_all - cols + extra if short else target * cols
         return (begin, extra, cols - extra) if short else (begin, 0, cols)
 
-    def own_piece(kind, target):
+    def part_rows(kind, target, part, side):
+        _, _, size = piece_bounds(target)
+        whole = half_d if kind < 2 else size // 2
+        rows_here = whole // PARTS
+        return pl.multiple_of(side * whole + part * rows_here, 16), rows_here
+
+    def own_piece(kind, target, part):
         src = (gate_ref, up_ref, down_ref)[kind]
         begin, _, size = piece_bounds(target)
+        first, count = part_rows(kind, target, part, y)
         if kind < 2:
-            return src.at[d_half, pl.ds(begin, size)]
-        return src.at[pl.ds(pl.multiple_of(begin + y * (size // 2), 64), size // 2), :]
-
-    def final_place(kind, source, target):
+            return src.at[pl.ds(first, count), pl.ds(begin, size)]
+        return src.at[pl.ds(pl.multiple_of(begin + first, 16), count), :]
+
+    def final_place(kind, source, target, part, side):
         dst = (wg, wu, wd)[kind]
         _, skip, size = piece_bounds(target)
+        first, count = part_rows(kind, target, part, side)
         if kind < 2:
-            return dst.at[source, d_half, pl.ds(skip, size)]
-        return dst.at[source, pl.ds(pl.multiple_of(skip + y * (size // 2), 64), size // 2)]
-
-    def transit_place(kind, here, source, target):
+            return dst.at[source, pl.ds(first, count), pl.ds(skip, size)]
+        return dst.at[source, pl.ds(pl.multiple_of(skip + first, 16), count)]
+
+    def transit_place(kind, here, source, target, part):
         buffer = (tg, tu, td)[kind].at[transit_slot(here, source, target)]
         _, _, size = piece_bounds(target)
-        return buffer.at[:, pl.ds(0, size)] if kind < 2 else buffer.at[pl.ds(0, size // 2)]
-
-    def weight_hop(kind, here, source, target):
+        first, count = part_rows(kind, target, part, 0)
+        return buffer.at[pl.ds(first, count), pl.ds(0, size)] if kind < 2 else buffer.at[pl.ds(first, count)]
+
+    def weight_hop(kind, here, source, target, part):
         there = here + 1 if target > here else here - 1
         if source == here:
-            piece, ssem = own_piece(kind, target), w_ss.at[kind, target]
+            piece, ssem = own_piece(kind, target, part), w_ss.at[kind // 2]
         else:
-            piece, ssem = transit_place(kind, here, source, target), t_ss.at[kind, transit_slot(here, source, target)]
+            piece = transit_place(kind, here, source, target, part)
+            ssem = t_ss.at[kind // 2]
         if there == target:
-            place, rsem = final_place(kind, source, target), w_rs.at[kind, source]
+            place, rsem = final_place(kind, source, target, part, y), w_rs.at[kind, PARTS * source + part]
         else:
-            place, rsem = transit_place(kind, there, source, target), t_rs.at[kind, transit_slot(there, source, target)]
+            place = transit_place(kind, there, source, target, part)
+            rsem = t_rs.at[kind, PARTS * transit_slot(there, source, target) + part]
         return remote(piece, place, ssem, rsem, sp=there)
 
     def move_weights(kinds, here, source, target):
         for kind in kinds:
-            if source != here:
-                before = here - 1 if source < here else here + 1
-                with scoped(f"pass{kind}_{source}{target}"):
-                    weight_hop(kind, before, source, target).wait_recv()
-            weight_hop(kind, here, source, target).start()
-
-    def weight_hand(kind, source, target):
-        place = final_place(kind, source, target)
-        return remote(place, place, f_ss.at[kind, source], f_rs.at[kind, source], grp=1 - y)
+            for part in range(PARTS):
+                if source != here:
+                    before = here - 1 if source < here else here + 1
+                    with scoped(f"pass{kind}{part}_{source}{target}"):
+                        weight_hop(kind, before, source, target, part).wait_recv()
+                weight_hop(kind, here, source, target, part).start()
+
+    def weight_hand(kind, source, target, part):
+        place = final_place(kind, source, target, part, y)
+        return remote(place, place, f_ss.at[kind // 2], f_rs.at[kind, PARTS * source + part], grp=1 - y)
 
     def hand_over(kinds, here, source):
         for kind in kinds:
-            before = here - 1 if source < here else here + 1
-            with scoped(f"hand{kind}_{source}"):
-                weight_hop(kind, before, source, here).wait_recv()
-            weight_hand(kind, source, here).start()
+            for part in range(PARTS):
+                before = here - 1 if source < here else here + 1
+                with scoped(f"hand{kind}{part}_{source}"):
+                    weight_hop(kind, before, source, here, part).wait_recv()
+                weight_hand(kind, source, here, part).start()
 
     def own_copy(kind, short):
         src, dst = ((gate_ref, wg), (up_ref, wu), (down_ref, wd))[kind]
@@ -402,7 +413,7 @@
 
     def act_z(row, begin, target, way):
         piece = act.at[t, row]
-        return remote(piece, piece, az_ss.at[way, row], az_rs.at[row], sp=target)
+        return remote(piece, piece, az_ss.at[way], az_rs.at[row], sp=target)
 
     def along(here, row, action):
         if row <= here < last:
@@ -412,11 +423,11 @@
 
     def act_x(row):
         piece = act.at[t, row]
-        return remote(piece, piece, ax_ss.at[row], ax_rs.at[row], tp=xpeer)
+        return remote(piece, piece, ax_ss.at[0], ax_rs.at[row], tp=xpeer)
 
     def act_c(row, second):
         piece = act.at[xpeer if second else t, row]
-        return remote(piece, piece, ac_ss.at[second, row], ac_rs.at[second, row], tp=cpeer)
+        return remote(piece, piece, ac_ss.at[0], ac_rs.at[second, row], tp=cpeer)
 
     def start(copy):
         copy.start()
@@ -488,10 +499,9 @@
     gains[t] = jnp.broadcast_to(gain_ref[...].reshape(1, blk), gains.shape[1:])
     gain_copies = []
     for k in others:
-        copy = remote(gains.at[t], gains.at[t], g_ss.at[k], g_rs.at[k], tp=flip(t, k))
+        copy = remote(gains.at[t], gains.at[t], g_ss.at[0], g_rs.at[k - 1], tp=flip(t, k))
         copy.start()
         gain_copies.append(copy)
-        sends.append(copy)
 
     q_refs = (q1_ref, q2_ref)
     lane = lax.broadcasted_iota(jnp.int32, (1, 2 * widths[0]), 1)
@@ -563,8 +573,7 @@
         mp[1] = project(dpeer).astype(jnp.bfloat16)
         to_core = remote(mp.at[pl.ds(0, 2)], rsb.at[pl.ds(0, 2)], rs_ss.at[0], rs_rs.at[0], tp=cpeer)
         to_core.start()
-        to_x = remote(mp.at[2], rsb.at[2], rs_ss.at[1], rs_rs.at[1], tp=xpeer)
-        sends.extend((to_core, to_x))
+        to_x = remote(mp.at[2], rsb.at[2], rs_ss.at[0], rs_rs.at[1], tp=xpeer)
         mine_ref[1] = project(xpeer)
         mine_ref[0] = residual_ref[...].astype(jnp.float32) + project(t)
     next_step()
@@ -590,23 +599,16 @@
     for copy in gain_copies:
         copy.wait_recv()
 
-    def place_of(kind, source, short):
-        size = cols - extra if short else cols
-        skip = extra if short else 0
-        if kind < 2:
-            half = pl.ds(pl.multiple_of((1 - y) * half_d, half_d), half_d)
-            return (wg, wu)[kind].at[source, half, pl.ds(skip, size)]
-        part = (1 - y) * (size // 2)
-        return wd.at[source, pl.ds(pl.multiple_of(skip + part, 64), size // 2)]
-
     def await_weights(kinds, source):
         def go(short):
             for kind in kinds:
-                place = place_of(kind, source, short)
 
                 @pl.when(source != s)
-                def _(kind=kind, place=place):
-                    remote(place, place, f_ss.at[kind, source], f_rs.at[kind, source], grp=1 - y).wait_recv()
+                def _(kind=kind):
+                    for part in range(PARTS):
+                        place = final_place(kind, source, last if short else 0, part, 1 - y)
+                        sem = PARTS * source + part
+                        remote(place, place, f_ss.at[kind // 2], f_rs.at[kind, sem], grp=1 - y).wait_recv()
 
                 @pl.when(source == s)
                 def _(kind=kind):
@@ -642,12 +644,17 @@
             hidden = gate / (1.0 + jnp.exp(-gate)) * up
             hid[k] = jnp.where(mine, hidden, 0.0).astype(jnp.bfloat16)
 
-    r1a, r1b, r2 = {}, {}, {}
+    r1a, r1b, r2, r3 = {}, {}, {}, {}
+    half_rows = rows // 2
     for k in everyone:
-        r1a[k] = remote(c1.at[k, 1], c1r.at[k, 1], c_ss.at[0, k], c_rs.at[0, k], tp=cpeer)
-        r1b[k] = remote(c1.at[k, 0], c1r.at[k, 0], c_ss.at[3, k], c_rs.at[3, k], tp=cpeer)
-        r2[k] = remote(c2.at[k], c2r.at[k], c_ss.at[1, k], c_rs.at[1, k], tp=xpeer)
-    r3 = {k: remote(c3.at[k], c3r.at[k], c_ss.at[2, k], c_rs.at[2, k], sp=flip(s, k - 2 if k == 3 else k)) for k in others}
+        r1a[k] = remote(c1.at[k, 1], c1r.at[k, 1], c_ss.at[0], c_rs.at[0, k], tp=cpeer)
+        r1b[k] = remote(c1.at[k, 0], c1r.at[k, 0], c_ss.at[0], c_rs.at[1, k], tp=cpeer)
+        for h in range(2):
+            some = pl.ds(h * half_rows, half_rows)
+            r2[k, h] = remote(c2.at[k, some], c2r.at[k, some], c_ss.at[1], c_rs.at[2 + h, k], tp=xpeer)
+            if k:
+                target = flip(s, 1 if k == 3 else k)
+                r3[k, h] = remote(c3.at[k, some], c3r.at[k, some], c_ss.at[2], c_rs.at[4 + h, k], sp=target)
 
     def cross(k):
         next_step()
@@ -660,8 +667,10 @@
         next_step()
         with scoped(f"r1a{k}"):
             r1a[k].wait_recv()
-        c2[k] = (po[k, 1] + c1r[k, 1].astype(jnp.float32)).astype(jnp.bfloat16)
-        r2[k].start()
+        for h in range(2):
+            some = pl.ds(h * half_rows, half_rows)
+            c2[k, some] = (po[k, 1, some] + c1r[k, 1, some].astype(jnp.float32)).astype(jnp.bfloat16)
+            r2[k, h].start()
 
     def near(k):
         next_step()
@@ -670,22 +679,24 @@
             r1b[k].start()
             po[k, 0] = dot(hid[k], wd[t])
 
-    def finish_row(k):
+    def finish_row(k, h):
         next_step()
-        with scoped(f"r1b{k}"):
-            r1b[k].wait_recv()
-        with scoped(f"r2_{k}"):
-            r2[k].wait_recv()
-        result = po[k, 0] + c1r[k, 0].astype(jnp.float32) + c2r[k].astype(jnp.float32)
+        some = pl.ds(h * half_rows, half_rows)
+        if h == 0:
+            with scoped(f"r1b{k}"):
+                r1b[k].wait_recv()
+        with scoped(f"r2_{k}{h}"):
+            r2[k, h].wait_recv()
+        result = po[k, 0, some] + c1r[k, 0, some].astype(jnp.float32) + c2r[k, some].astype(jnp.float32)
         if k == 2:
-            with scoped("r3_3"):
-                r3[3].wait_recv()
-            result = result + c3r[3].astype(jnp.float32)
+            with scoped(f"r3_3{h}"):
+                r3[3, h].wait_recv()
+            result = result + c3r[3, some].astype(jnp.float32)
         if k:
-            c3[k] = result.astype(jnp.bfloat16)
-            r3[k].start()
+            c3[k, some] = result.astype(jnp.bfloat16)
+            r3[k, h].start()
         else:
-            po[0, 0] = result
+            po[0, 0, some] = result
 
     hidden_of(3)
     next_step()
@@ -699,30 +710,45 @@
     hidden_of(1)
     to_other_chip(2)
     cross(1)
-    hidden_of(0)
-    to_other_chip(1)
-    cross(0)
-    to_other_chip(0)
     next_step()
     with scoped("await_near"):
         await_weights((2,), cpeer)
         await_weights((2,), t)
     near(3)
+    hidden_of(0)
+    to_other_chip(1)
+    finish_row(3, 0)
+    cross(0)
+    finish_row(3, 1)
+    to_other_chip(0)
     near(2)
-    finish_row(3)
+    finish_row(2, 0)
+    finish_row(2, 1)
     near(1)
     near(0)
-    finish_row(2)
-    finish_row(1)
-    finish_row(0)
+    finish_row(1, 0)
+    finish_row(1, 1)
+    finish_row(0, 0)
+    finish_row(0, 1)
 
     next_step()
-    ffn = po[0, 0]
-    for k in (1, 2):
-        with scoped(f"r3_{k}"):
-            r3[k].wait_recv()
-        ffn = ffn + c3r[k].astype(jnp.float32)
-    out_ref[...] = (stream[...] + 0.5 * ffn).astype(jnp.bfloat16)
+    for h in range(2):
+        some = pl.ds(h * half_rows, half_rows)
+        for k in (1, 2):
+            with scoped(f"r3_{k}{h}"):
+                r3[k, h].wait_recv()
+        ffn = po[0, 0, some] + c3r[1, some].astype(jnp.float32) + c3r[2, some].astype(jnp.float32)
+        out_ref[some, :] = (stream[some, :] + 0.5 * ffn).astype(jnp.bfloat16)
+
+    def sent(ref, sem):
+        remote(ref, ref, sem, rs_rs.at[0], tp=cpeer).wait_send()
+
+    def weights_sent(sems, width):
+        sent(gate_ref.at[:, pl.ds(0, width)], sems.at[0])
+        sent(down_ref.at[pl.ds(0, width // 2), :], sems.at[1])
+
+    def width_of(target):
+        return piece_bounds(target)[2]
 
     with scoped("drain"):
         for here in everyone:
@@ -730,27 +756,29 @@
             @pl.when(s == here)
             def _(here=here):
                 if here < last:
-                    for back in range(here + 1):
-                        for copy in kv_copies(back):
-                            copy.wait_send()
-                for kind in range(3):
-                    for there in everyone:
-                        if there != here:
-                            weight_hop(kind, here, here, there).wait_send()
-                            weight_hand(kind, there, here).wait_send()
-                    for source in everyone:
-                        for target in everyone:
-                            if min(source, target) < here < max(source, target):
-                                weight_hop(kind, here, source, target).wait_send()
-                for row in everyone:
-                    along(here, row, lambda copy: copy.wait_send())
-
-        for row in everyone:
-            sends.extend((act_x(row), act_c(row, 0), act_c(row, 1)))
-        for copies in (r1a, r1b, r2, r3):
-            sends.extend(copies.values())
-        for copy in sends:
-            copy.wait_send()
+                    for i, buffer in enumerate((k1b, k2b, vb)):
+                        sent(buffer.at[pl.ds(0, here + 1)], kv_ss.at[i])
+                    sent(act.at[0, pl.ds(0, here + 1)], az_ss.at[0])
+                if here:
+                    sent(act.at[0, pl.ds(0, sp_count - here)], az_ss.at[1])
+                weights_sent(w_ss, sum(width_of(there) for there in everyone if there != here))
+                weights_sent(f_ss, (sp_count - 1) * width_of(here))
+                through = [
+                    width_of(target)
+                    for source in everyone
+                    for target in everyone
+                    if min(source, target) < here < max(source, target)
+                ]
+                if through:
+                    weights_sent(t_ss, sum(through))
+
+        sent(act.at[0], ax_ss.at[0])
+        sent(act.at[pl.ds(0, 2)], ac_ss.at[0])
+        sent(gains.at[pl.ds(0, sp_count - 1)], g_ss.at[0])
+        sent(mp, rs_ss.at[0])
+        sent(c1, c_ss.at[0])
+        sent(c2, c_ss.at[1])
+        sent(c3.at[pl.ds(0, sp_count - 1)], c_ss.at[2])
 
 
 def fits(axes, query_first, values, lambdas, residual, gate_weight):
@@ -766,7 +794,7 @@
     cols = -(-hidden_all // (128 * sp)) * 128
     if cols * sp - hidden_all >= cols or cols > hidden_all:
         return False
-    if (cols * sp - hidden_all) % 128 or blk % 32:
+    if (cols * sp - hidden_all) % 128 or blk % 64 or rows % 32:
         return False
     need = 6 * sp * blk * cols + rows * blk * 2 * 20 * sp
     return need < 40 * 1024 * 1024
@@ -846,27 +874,27 @@
             pltpu.VMEM((n, rows, blk), bf16),
             pltpu.VMEM((n, rows, blk), bf16),
             pltpu.VMEM((n, rows, blk), bf16),
-            dma((3, n)),
-            dma((3, n)),
-            dma((3, n)),
-            dma((3, n)),
-            dma((3, n)),
-            dma((3, n)),
-            dma((3, n)),
-            dma((3, n)),
+            dma((3,)),
+            dma((3, n - 1)),
+            dma((2,)),
+            dma((3, PARTS * n)),
+            dma((2,)),
+            dma((3, PARTS * n)),
+            dma((2,)),
+            dma((3, PARTS * n)),
             dma((4,)),
-            dma((n,)),
-            dma((n,)),
+            dma((1,)),
+            dma((n - 1,)),
+            dma((1,)),
             dma((2,)),
             dma((2,)),
+            dma((n,)),
+            dma((1,)),
+            dma((n,)),
+            dma((1,)),
             dma((2, n)),
-            dma((n,)),
-            dma((n,)),
-            dma((n,)),
-            dma((2, n)),
-            dma((2, n)),
-            dma((4, n)),
-            dma((4, n)),
+            dma((3,)),
+            dma((6, n)),
         ],
         compiler_params=pltpu.CompilerParams(
             collective_id=0, has_side_effects=True, vmem_limit_bytes=60 * 1024 * 1024

time: 102 us -> 98.9 us (0.970)
  the two profiles are of different devices: /device:TPU:18 before, /device:TPU:1 now
where the time goes in v2:
time: 98.9 us; the launch traced here: 97.8 us
  Pallas kernels  96.2 us (97%)
  local copies, waits for them, and re-layouts  1.62 us (2%)
    pallas_call x1, Pallas kernels, one_device(): pl.pallas_call(functools.partial(layer_kernel, n, widths), out_shape=jax....  96.2 us

profile of v2, /device:TPU:1, one launch (start us, length us, event | category | flops | bytes accessed | tf_op | source)
XLA Modules:
  0.0 97.8 jit_solution(5137245197099547714)
XLA Ops:
  0.0 96.2 %shard_map.118 = bf16[192,512]{1,0:T(8,128)(2,1)} custom-call(bf16[192,128]{1,0:T(8,128)(2,1)} %q1_ref.1, bf16[192,256]{1,0:T(8,128)(2,1)} %q2_ref.1, bf16[192,128]{1,0:T(8,128)(2,1)} %k1_ref.1, bf16[192,256]{1,0:T(8,128)(2,1)} %k2_ref.1, bf16[192,2,128]{2,1,0:T(2,128)(2,1)} %v_ref.1, f32[1,2]{1,0:T(1,128)} %bitcast.1, bf16[192,512]{1,0:T(8,128)(2,1)} %residual_ref.1, ...), custom_call_target="tpu_custom_call" | custom-call | tf_op jit(solution)/shard_map/pallas_call | solution.py:844
  96.2 1.6 %copy.14 = bf16[192,512]{1,0:T(8,128)(2,1)} copy(bf16[192,512]{1,0:T(8,128)(2,1)} %shard_map.118) | data formatting | bytes 393216

commit v3 on v2

--- a/solution.py
+++ b/solution.py
@@ -220,6 +220,19 @@
 def layer_kernel(
     sp_count,
     widths,
+    q1_hbm,
+    q2_hbm,
+    k1_hbm,
+    k2_hbm,
+    v_hbm,
+    lam_hbm,
+    residual_hbm,
+    gain_hbm,
+    proj_hbm,
+    gate_ref,
+    up_ref,
+    down_ref,
+    out_ref,
     q1_ref,
     q2_ref,
     k1_ref,
@@ -228,11 +241,6 @@
     lam_ref,
     residual_ref,
     gain_ref,
-    proj_hbm,
-    gate_ref,
-    up_ref,
-    down_ref,
-    out_ref,
     k1b,
     k2b,
     vb,
@@ -269,6 +277,7 @@
     f_ss,
     f_rs,
     own_sem,
+    in_sem,
     g_ss,
     g_rs,
     rs_ss,
@@ -312,8 +321,19 @@
         pl.semaphore_signal(barrier, inc=1, device_id={"sp": flip(s, k)}, device_id_type=pl.DeviceIdType.MESH)
         pl.semaphore_signal(barrier, inc=1, device_id={"tp": flip(t, k)}, device_id_type=pl.DeviceIdType.MESH)
     pl.semaphore_signal(barrier, inc=1, device_id={"grp": 1 - y}, device_id_type=pl.DeviceIdType.MESH)
-    with scoped("barrier"):
-        pl.semaphore_wait(barrier, 2 * (sp_count - 1) + 1)
+    inputs = (
+        (k1_hbm, k1_ref),
+        (k2_hbm, k2_ref),
+        (v_hbm, v_ref),
+        (q1_hbm, q1_ref),
+        (q2_hbm, q2_ref),
+        (gain_hbm, gain_ref),
+        (lam_hbm, lam_ref),
+        (residual_hbm, residual_ref),
+    )
+    loads = [pltpu.make_async_copy(far, here, in_sem.at[i]) for i, (far, here) in enumerate(inputs)]
+    for load in loads:
+        load.start()
 
     half_d = wg.shape[1] // 2
     extra = sp_count * cols - hidden_all
@@ -474,13 +494,6 @@
                         for event in events:
                             perform(here, event)
 
-    next_step()
-
-    @pl.when(s < last)
-    def _():
-        for copy in kv_copies(0):
-            copy.start()
-
     @pl.when(s == last)
     def _():
         wg[:, :, :extra] = jnp.zeros((sp_count, wg.shape[1], extra), jnp.bfloat16)
@@ -496,7 +509,18 @@
 
     either(s == last, start_own)
 
+    for load in loads[:-1]:
+        load.wait()
     gains[t] = jnp.broadcast_to(gain_ref[...].reshape(1, blk), gains.shape[1:])
+    with scoped("barrier"):
+        pl.semaphore_wait(barrier, 2 * (sp_count - 1) + 1)
+    next_step()
+
+    @pl.when(s < last)
+    def _():
+        for copy in kv_copies(0):
+            copy.start()
+
     gain_copies = []
     for k in others:
         copy = remote(gains.at[t], gains.at[t], g_ss.at[0], g_rs.at[k - 1], tp=flip(t, k))
@@ -555,6 +579,7 @@
 
     next_step()
     proj_copy.wait()
+    loads[-1].wait()
     with scoped("finish"):
         attended = []
         for group in range(2):
@@ -838,15 +863,22 @@
     widths = (query_first.shape[1] // 2, query_second.shape[1] // 2)
     bf16, f32 = jnp.bfloat16, jnp.float32
     vmem = pl.BlockSpec(memory_space=pltpu.VMEM)
-    smem = pl.BlockSpec(memory_space=pltpu.SMEM)
     hbm = pl.BlockSpec(memory_space=pl.ANY)
     dma = pltpu.SemaphoreType.DMA
     return pl.pallas_call(
         functools.partial(layer_kernel, n, widths),
         out_shape=jax.ShapeDtypeStruct((rows, blk), bf16),
-        in_specs=[vmem] * 5 + [smem, vmem, vmem] + [hbm] * 4,
+        in_specs=[hbm] * 12,
         out_specs=vmem,
         scratch_shapes=[
+            pltpu.VMEM(query_first.shape, bf16),
+            pltpu.VMEM(query_second.shape, bf16),
+            pltpu.VMEM(key_first.shape, bf16),
+            pltpu.VMEM(key_second.shape, bf16),
+            pltpu.VMEM(values.shape, bf16),
+            pltpu.SMEM(lambdas.T.shape, f32),
+            pltpu.VMEM(residual.shape, bf16),
+            pltpu.VMEM(norm_gain.shape, bf16),
             pltpu.VMEM((n,) + key_first.shape, bf16),
             pltpu.VMEM((n,) + key_second.shape, bf16),
             pltpu.VMEM((n,) + values.shape, bf16),
@@ -883,6 +915,7 @@
             dma((2,)),
             dma((3, PARTS * n)),
             dma((4,)),
+            dma((8,)),
             dma((1,)),
             dma((n - 1,)),
             dma((1,)),

time: 98.9 us -> 97.8 us (0.989)
  Pallas kernels: 96.2 us -> 95.1 us
    pallas_call x1, Pallas kernels: 96.2 us -> 95.1 us  [one_device(): pl.pallas_call(functools.partial(layer_kernel, n, widths), out_shape=jax....]
where the time goes in v3:
time: 97.8 us; the launch traced here: 96.7 us
  Pallas kernels  95.1 us (97%)
  local copies, waits for them, and re-layouts  1.62 us (2%)
    pallas_call x1, Pallas kernels, one_device(): pl.pallas_call(functools.partial(layer_kernel, n, widths), out_shape=jax....  95.1 us

profile of v3, /device:TPU:1, one launch (start us, length us, event | category | flops | bytes accessed | tf_op | source)
XLA Modules:
  0.0 96.7 jit_solution(16286952499971777594)
XLA Ops:
  0.0 95.1 %shard_map.118 = bf16[192,512]{1,0:T(8,128)(2,1)} custom-call(bf16[192,128]{1,0:T(8,128)(2,1)} %q1_hbm.1, bf16[192,256]{1,0:T(8,128)(2,1)} %q2_hbm.1, bf16[192,128]{1,0:T(8,128)(2,1)} %k1_hbm.1, bf16[192,256]{1,0:T(8,128)(2,1)} %k2_hbm.1, bf16[192,2,128]{2,1,0:T(2,128)(2,1)} %v_hbm.1, f32[1,2]{1,0:T(1,128)} %bitcast.1, bf16[192,512]{1,0:T(8,128)(2,1)} %residual_hbm.1, ...), custom_call_target="tpu_custom_call" | custom-call | tf_op jit(solution)/shard_map/pallas_call | solution.py:868
  95.1 1.6 %copy.14 = bf16[192,512]{1,0:T(8,128)(2,1)} copy(bf16[192,512]{1,0:T(8,128)(2,1)} %shard_map.118) | data formatting | bytes 393216

commit v4 on v3

--- a/solution.py
+++ b/solution.py
@@ -128,55 +128,85 @@
 
 PLAN = (
     {
-        (1, 0): ((0, 1, 0),),
-        (1, 1): ((1, 1, 3), (0, 1, 0)),
-        (2, 0): ((0, 2, 0), (1, 2, 1), (1, 2, 3), (1, 2, 0)),
-        (2, 1): ((0, 2, 3), (1, 2, 1), (0, 2, 0), (1, 2, 0)),
-        (3, 0): ((1, 3, 0), (0, 3, 0), (0, 3, 1), (0, 3, 2), (1, 3, 2)),
-        (3, 1): ((0, 3, 0), (1, 3, 0), (0, 3, 2), (1, 3, 1)),
+        (1, 0): ((1, 1, 0), (0, 1, 0)),
+        (1, 1): ((0, 1, 0),),
+        (2, 0): ((0, 2, 0), (0, 2, 1)),
+        (2, 1): ((0, 2, 0), (0, 2, 1), (1, 2, 0)),
+        (3, 0): ((0, 3, 1), (0, 3, 0), (0, 3, 2), (1, 3, 0)),
+        (3, 1): ((0, 3, 2), (1, 3, 0), (0, 3, 0)),
+    },
+    {
+        (0, 0): ((0, 0, 1),),
+        (1, 0): ((0, 1, 2),),
+        (1, 1): ((0, 1, 2), (0, 2, 0), (1, 0, 3)),
+        (2, 0): ((0, 3, 1), (1, 2, 3), (0, 2, 3)),
     },
     {
         (0, 0): ((0, 0, 2),),
-        (0, 1): ((0, 0, 1),),
-        (1, 0): ((0, 1, 3),),
-        (2, 0): ((0, 2, 1),),
-        (2, 1): ((0, 3, 0), (1, 1, 3)),
-    },
-    {
-        (1, 1): ((0, 1, 2), (0, 2, 0)),
-        (2, 0): ((1, 3, 0),),
-        (2, 1): ((0, 2, 1), (2, 3)),
+        (1, 0): ((0, 1, 3), (0, 2, 0)),
+        (2, 1): ((2, 3), (0, 2, 3)),
         (3, 1): ((0, 3, 1),),
     },
     {
-        (0, 0): ((1, 0, 3),),
-        (0, 1): ((2, 1),),
-        (1, 0): ((0, 1, 2), (0, 2, 0)),
-        (1, 1): ((1, 2, 0), (3, 2), (0, 1, 3)),
-        (2, 0): ((0, 1, 3), (0, 2, 3), (0, 3, 0), (2, 3)),
-    },
-    {
-        (0, 0): ((2, 1), (0, 0, 3), (2, 2), (4, 1), (0, 0, 1), (3, 3), (1, 0, 2), (5, 1), (1, 0, 1), (2, 3), (4, 2), (4, 3), (3, 2), (5, 0), (3, 1), (5, 2), (5, 3)),
-        (0, 1): ((0, 0, 2), (5, 0), (1, 0, 3), (1, 0, 1), (4, 1), (5, 1), (0, 0, 3), (2, 2), (1, 0, 2), (3, 2), (3, 1), (2, 3), (3, 3), (4, 2), (4, 3), (5, 2), (5, 3)),
-        (1, 0): ((4, 0), (1, 1, 0), (0, 0, 3), (3, 2), (1, 3, 0), (0, 0, 2), (2, 2), (1, 0, 3), (0, 3, 0), (2, 0), (4, 2), (4, 3), (1, 0, 2), (1, 2, 0), (1, 1, 3), (1, 1, 2), (2, 3), (5, 1), (3, 3), (3, 0), (5, 2), (5, 3), (5, 0)),
-        (1, 1): ((4, 0), (1, 1, 0), (0, 0, 2), (2, 0), (0, 3, 0), (5, 1), (1, 1, 2), (4, 2), (2, 2), (0, 0, 3), (3, 0), (1, 3, 0), (4, 3), (5, 0), (1, 0, 3), (1, 0, 2), (2, 3), (5, 2), (3, 3), (5, 3)),
-        (2, 0): ((2, 1), (4, 0), (4, 3), (5, 0), (0, 0, 3), (3, 3), (0, 3, 1), (5, 2), (4, 1), (2, 0), (1, 3, 1), (5, 3), (3, 0), (1, 0, 3), (5, 1)),
-        (2, 1): ((1, 3, 0), (4, 1), (2, 1), (4, 0), (4, 3), (1, 2, 3), (2, 0), (0, 3, 1), (0, 1, 3), (1, 3, 1), (5, 0), (3, 3), (3, 1), (5, 2), (5, 3), (0, 0, 3)),
-        (3, 0): ((1, 3, 1), (2, 2), (3, 2), (4, 2), (4, 0), (2, 1), (2, 0), (4, 1), (5, 0), (3, 0)),
-        (3, 1): ((1, 3, 2), (4, 2), (3, 1), (2, 2), (4, 0), (4, 1), (3, 2), (2, 1), (5, 0), (5, 2), (2, 0), (3, 0), (5, 3), (5, 1)),
-    },
-    {
-        (2, 1): ((1, 0, 3), (5, 1), (3, 0)),
-    },
-    {
-        (3, 0): ((5, 1), (3, 1)),
-    },
-    {
-        (3, 0): ((5, 3), (5, 2)),
-    },
-    {
-        (2, 0): ((1, 1, 3),),
-    },
+        (0, 1): ((1, 0, 3), (0, 0, 1)),
+        (1, 1): ((1, 1, 0),),
+        (2, 0): ((0, 3, 0), (2, 1), (0, 1, 3), (2, 3)),
+        (2, 1): ((1, 2, 1), (2, 1), (1, 0, 3)),
+        (3, 0): ((2, 2), (3, 2)),
+    },
+    {
+        (0, 0): ((0, 0, 3), (2, 2), (5, 0), (1, 0, 3), (4, 1), (1, 0, 2), (2, 3), (2, 1), (1, 0, 1), (4, 2), (4, 3), (3, 2), (5, 2), (5, 1), (5, 3)),
+        (0, 1): ((1, 0, 1), (0, 0, 3), (0, 0, 2), (2, 2), (5, 1), (1, 0, 2), (2, 1), (3, 1), (4, 2), (2, 3), (4, 1), (5, 0), (4, 3), (5, 3), (3, 2), (5, 2)),
+        (1, 0): ((2, 2), (4, 0), (0, 0, 2), (2, 0), (0, 3, 0), (2, 3), (4, 2), (0, 0, 3), (5, 1), (1, 1, 3), (1, 0, 3), (1, 0, 2), (4, 3), (5, 2), (3, 0), (5, 0), (1, 2, 0)),
+        (1, 1): ((4, 0), (0, 1, 3), (2, 0), (3, 0), (4, 2), (0, 0, 3), (2, 2), (0, 3, 0), (0, 0, 2), (4, 3), (1, 0, 2), (1, 2, 0), (1, 1, 3), (5, 2), (1, 1, 2), (2, 3), (1, 3, 0), (3, 2), (5, 3)),
+        (2, 0): ((4, 3), (5, 1), (4, 1), (4, 0), (1, 2, 0), (5, 2), (1, 2, 1), (2, 0), (5, 0), (1, 3, 0), (0, 0, 3)),
+        (2, 1): ((0, 3, 0), (4, 1), (4, 0), (1, 2, 3), (5, 2), (4, 3), (0, 3, 1), (1, 3, 0), (0, 1, 3), (0, 0, 3), (2, 0), (5, 1), (3, 0), (5, 0)),
+        (3, 0): ((4, 1), (1, 3, 1), (5, 3), (2, 1), (4, 0), (2, 0), (5, 2), (1, 3, 2), (4, 2), (5, 0), (5, 1)),
+        (3, 1): ((1, 3, 2), (2, 2), (4, 2), (4, 1), (3, 0), (3, 2), (1, 3, 1), (4, 0), (2, 1), (2, 0), (5, 1), (5, 0)),
+    },
+    {
+        (1, 0): ((1, 1, 2),),
+        (2, 1): ((1, 3, 1),),
+    },
+    {
+        (1, 0): ((3, 2), (1, 3, 0), (5, 3)),
+        (2, 1): ((5, 3), (3, 3), (1, 1, 3)),
+    },
+    {
+        (3, 1): ((5, 2),),
+    },
+    {
+        (1, 1): ((5, 1), (5, 0)),
+        (2, 0): ((5, 3), (1, 1, 3)),
+    },
+    {
+        (0, 0): ((3, 3),),
+        (2, 0): ((1, 0, 3), (1, 3, 1)),
+        (3, 1): ((5, 3),),
+    },
+    {},
+    {
+        (0, 1): ((3, 3),),
+        (3, 0): ((3, 0), (3, 1)),
+    },
+    {
+        (1, 0): ((3, 3),),
+        (2, 1): ((3, 1),),
+    },
+    {
+        (2, 0): ((3, 0), (3, 3)),
+        (3, 1): ((3, 1),),
+    },
+    {},
+    {
+        (0, 0): ((3, 1),),
+        (1, 1): ((3, 3),),
+    },
+    {},
+    {},
+    {},
+    {},
+    {},
     {},
     {},
     {},
@@ -202,6 +232,51 @@
     {},
     {},
     {},
+    {},
+    {},
+)
+
+TAIL = (
+    ("hidden", 3),
+    ("await_far", 0),
+    ("far", 0, 3),
+    ("hidden", 2),
+    ("cross", 0, 3),
+    ("far", 0, 2),
+    ("hidden", 1),
+    ("cross", 0, 2),
+    ("far", 0, 1),
+    ("hidden", 0),
+    ("cross", 0, 1),
+    ("far", 0, 0),
+    ("cross", 0, 0),
+    ("await_near", 0),
+    ("near", 0, 3),
+    ("near", 0, 2),
+    ("settle", 0, 3),
+    ("near", 0, 1),
+    ("near", 0, 0),
+    ("await_far", 1),
+    ("far", 1, 3),
+    ("far", 1, 2),
+    ("cross", 1, 3),
+    ("settle", 0, 2),
+    ("far", 1, 1),
+    ("cross", 1, 2),
+    ("far", 1, 0),
+    ("cross", 1, 1),
+    ("cross", 1, 0),
+    ("await_near", 1),
+    ("near", 1, 3),
+    ("near", 1, 2),
+    ("settle", 0, 1),
+    ("settle", 1, 3),
+    ("near", 1, 1),
+    ("near", 1, 0),
+    ("settle", 0, 0),
+    ("settle", 1, 2),
+    ("settle", 1, 1),
+    ("settle", 1, 0),
 )
 
 WEIGHTS_IN, DOWN_IN, HAND_IN, HAND_DOWN, ROW, ACROSS = range(6)
@@ -649,7 +724,6 @@
 
     def hidden_of(k):
         row = flip(s, k)
-        next_step()
         with scoped(f"acwait{k}"):
             act_c(row, 0).wait_recv()
             act_c(row, 1).wait_recv()
@@ -669,101 +743,77 @@
             hidden = gate / (1.0 + jnp.exp(-gate)) * up
             hid[k] = jnp.where(mine, hidden, 0.0).astype(jnp.bfloat16)
 
-    r1a, r1b, r2, r3 = {}, {}, {}, {}
-    half_rows = rows // 2
+    core = t % 2
+    r1, r2, r3 = {}, {}, {}
     for k in everyone:
-        r1a[k] = remote(c1.at[k, 1], c1r.at[k, 1], c_ss.at[0], c_rs.at[0, k], tp=cpeer)
-        r1b[k] = remote(c1.at[k, 0], c1r.at[k, 0], c_ss.at[0], c_rs.at[1, k], tp=cpeer)
-        for h in range(2):
-            some = pl.ds(h * half_rows, half_rows)
-            r2[k, h] = remote(c2.at[k, some], c2r.at[k, some], c_ss.at[1], c_rs.at[2 + h, k], tp=xpeer)
+        for far in range(2):
+            r1[k, far] = remote(c1.at[k, far], c1r.at[k, far], c_ss.at[0], c_rs.at[far, k], tp=cpeer)
+        r2[k] = remote(c2.at[k], c2r.at[k], c_ss.at[1], c_rs.at[2, k], tp=xpeer)
+        if k:
+            r3[k] = remote(c3.at[k], c3r.at[k], c_ss.at[2], c_rs.at[3, k], sp=flip(s, 1 if k == 3 else k))
+
+    def block_of(wave, far):
+        return 2 * ((1 - x) if far else x) + wave
+
+    def product(wave, k, far):
+        with scoped(f"product{wave}{k}{far}"):
+            value = dot(hid[k], wd[block_of(wave, far)])
+
+            @pl.when(core == wave)
+            def _():
+                po[k, far] = value
+
+            @pl.when(core != wave)
+            def _():
+                c1[k, far] = value.astype(jnp.bfloat16)
+                r1[k, far].start()
+
+    def to_other_chip(wave, k):
+        @pl.when(core == wave)
+        def _():
+            with scoped(f"cross{wave}{k}"):
+                r1[k, 1].wait_recv()
+            c2[k] = (po[k, 1] + c1r[k, 1].astype(jnp.float32)).astype(jnp.bfloat16)
+            r2[k].start()
+
+    def settle(wave, k):
+        @pl.when(core == wave)
+        def _():
+            with scoped(f"settle{wave}{k}"):
+                r1[k, 0].wait_recv()
+                r2[k].wait_recv()
+            result = po[k, 0] + c1r[k, 0].astype(jnp.float32) + c2r[k].astype(jnp.float32)
+            if k == 2:
+                with scoped(f"pair{wave}"):
+                    r3[3].wait_recv()
+                result = result + c3r[3].astype(jnp.float32)
             if k:
-                target = flip(s, 1 if k == 3 else k)
-                r3[k, h] = remote(c3.at[k, some], c3r.at[k, some], c_ss.at[2], c_rs.at[4 + h, k], sp=target)
-
-    def cross(k):
+                c3[k] = result.astype(jnp.bfloat16)
+                r3[k].start()
+            else:
+                po[0, 0] = result
+
+    for name, *where in TAIL:
         next_step()
-        with scoped(f"cross{k}"):
-            c1[k, 1] = dot(hid[k], wd[dpeer]).astype(jnp.bfloat16)
-            r1a[k].start()
-            po[k, 1] = dot(hid[k], wd[xpeer])
-
-    def to_other_chip(k):
-        next_step()
-        with scoped(f"r1a{k}"):
-            r1a[k].wait_recv()
-        for h in range(2):
-            some = pl.ds(h * half_rows, half_rows)
-            c2[k, some] = (po[k, 1, some] + c1r[k, 1, some].astype(jnp.float32)).astype(jnp.bfloat16)
-            r2[k, h].start()
-
-    def near(k):
-        next_step()
-        with scoped(f"near{k}"):
-            c1[k, 0] = dot(hid[k], wd[cpeer]).astype(jnp.bfloat16)
-            r1b[k].start()
-            po[k, 0] = dot(hid[k], wd[t])
-
-    def finish_row(k, h):
-        next_step()
-        some = pl.ds(h * half_rows, half_rows)
-        if h == 0:
-            with scoped(f"r1b{k}"):
-                r1b[k].wait_recv()
-        with scoped(f"r2_{k}{h}"):
-            r2[k, h].wait_recv()
-        result = po[k, 0, some] + c1r[k, 0, some].astype(jnp.float32) + c2r[k, some].astype(jnp.float32)
-        if k == 2:
-            with scoped(f"r3_3{h}"):
-                r3[3, h].wait_recv()
-            result = result + c3r[3, some].astype(jnp.float32)
-        if k:
-            c3[k, some] = result.astype(jnp.bfloat16)
-            r3[k, h].start()
+        if name == "hidden":
+            hidden_of(where[0])
+        elif name in ("far", "near"):
+            product(*where, far=int(name == "far"))
+        elif name == "cross":
+            to_other_chip(*where)
+        elif name == "settle":
+            settle(*where)
         else:
-            po[0, 0, some] = result
-
-    hidden_of(3)
+            with scoped(f"{name}{where[0]}"):
+                await_weights((2,), block_of(where[0], name == "await_far"))
+
     next_step()
-    with scoped("await_cross"):
-        await_weights((2,), dpeer)
-        await_weights((2,), xpeer)
-    cross(3)
-    hidden_of(2)
-    to_other_chip(3)
-    cross(2)
-    hidden_of(1)
-    to_other_chip(2)
-    cross(1)
-    next_step()
-    with scoped("await_near"):
-        await_weights((2,), cpeer)
-        await_weights((2,), t)
-    near(3)
-    hidden_of(0)
-    to_other_chip(1)
-    finish_row(3, 0)
-    cross(0)
-    finish_row(3, 1)
-    to_other_chip(0)
-    near(2)
-    finish_row(2, 0)
-    finish_row(2, 1)
-    near(1)
-    near(0)
-    finish_row(1, 0)
-    finish_row(1, 1)
-    finish_row(0, 0)
-    finish_row(0, 1)
-
-    next_step()
-    for h in range(2):
-        some = pl.ds(h * half_rows, half_rows)
-        for k in (1, 2):
-            with scoped(f"r3_{k}{h}"):
-                r3[k, h].wait_recv()
-        ffn = po[0, 0, some] + c3r[1, some].astype(jnp.float32) + c3r[2, some].astype(jnp.float32)
-        out_ref[some, :] = (stream[some, :] + 0.5 * ffn).astype(jnp.bfloat16)
+    ffn = po[0, 0]
+    for k in (1, 2):
+        with scoped(f"r3_{k}"):
+            r3[k].wait_recv()
+        ffn = ffn + c3r[k].astype(jnp.float32)
+    out_ref[...] = (stream[...] + 0.5 * ffn).astype(jnp.bfloat16)
 
     def sent(ref, sem):
         remote(ref, ref, sem, rs_rs.at[0], tp=cpeer).wait_send()
@@ -927,7 +977,7 @@
             dma((1,)),
             dma((2, n)),
             dma((3,)),
-            dma((6, n)),
+            dma((4, n)),
         ],
         compiler_params=pltpu.CompilerParams(
             collective_id=0, has_side_effects=True, vmem_limit_bytes=60 * 1024 * 1024

time: 97.8 us -> 95.8 us (0.980)
  Pallas kernels: 95.1 us -> 94 us
    pallas_call x1, Pallas kernels: 95.1 us -> 94 us  [one_device(): pl.pallas_call(functools.partial(layer_kernel, n, widths), out_shape=jax....]
where the time goes in v4:
time: 95.8 us; the launch traced here: 95.6 us
  Pallas kernels  94 us (98%)
  local copies, waits for them, and re-layouts  1.62 us (2%)
    pallas_call x1, Pallas kernels, one_device(): pl.pallas_call(functools.partial(layer_kernel, n, widths), out_shape=jax....  94 us

profile of v4, /device:TPU:1, one launch (start us, length us, event | category | flops | bytes accessed | tf_op | source)
XLA Modules:
  0.0 95.6 jit_solution(15655878396263591246)
XLA Ops:
  0.0 94.0 %shard_map.118 = bf16[192,512]{1,0:T(8,128)(2,1)} custom-call(bf16[192,128]{1,0:T(8,128)(2,1)} %q1_hbm.1, bf16[192,256]{1,0:T(8,128)(2,1)} %q2_hbm.1, bf16[192,128]{1,0:T(8,128)(2,1)} %k1_hbm.1, bf16[192,256]{1,0:T(8,128)(2,1)} %k2_hbm.1, bf16[192,2,128]{2,1,0:T(2,128)(2,1)} %v_hbm.1, f32[1,2]{1,0:T(1,128)} %bitcast.1, bf16[192,512]{1,0:T(8,128)(2,1)} %residual_hbm.1, ...), custom_call_target="tpu_custom_call" | custom-call | tf_op jit(solution)/shard_map/pallas_call | solution.py:918
  94.0 1.6 %copy.14 = bf16[192,512]{1,0:T(8,128)(2,1)} copy(bf16[192,512]{1,0:T(8,128)(2,1)} %shard_map.118) | data formatting | bytes 393216

commit v5 on v4

--- a/solution.py
+++ b/solution.py
@@ -128,91 +128,88 @@
 
 PLAN = (
     {
-        (1, 0): ((1, 1, 0), (0, 1, 0)),
-        (1, 1): ((0, 1, 0),),
-        (2, 0): ((0, 2, 0), (0, 2, 1)),
-        (2, 1): ((0, 2, 0), (0, 2, 1), (1, 2, 0)),
-        (3, 0): ((0, 3, 1), (0, 3, 0), (0, 3, 2), (1, 3, 0)),
-        (3, 1): ((0, 3, 2), (1, 3, 0), (0, 3, 0)),
-    },
-    {
-        (0, 0): ((0, 0, 1),),
-        (1, 0): ((0, 1, 2),),
-        (1, 1): ((0, 1, 2), (0, 2, 0), (1, 0, 3)),
-        (2, 0): ((0, 3, 1), (1, 2, 3), (0, 2, 3)),
-    },
-    {
-        (0, 0): ((0, 0, 2),),
-        (1, 0): ((0, 1, 3), (0, 2, 0)),
-        (2, 1): ((2, 3), (0, 2, 3)),
-        (3, 1): ((0, 3, 1),),
-    },
-    {
-        (0, 1): ((1, 0, 3), (0, 0, 1)),
-        (1, 1): ((1, 1, 0),),
-        (2, 0): ((0, 3, 0), (2, 1), (0, 1, 3), (2, 3)),
-        (2, 1): ((1, 2, 1), (2, 1), (1, 0, 3)),
-        (3, 0): ((2, 2), (3, 2)),
-    },
-    {
-        (0, 0): ((0, 0, 3), (2, 2), (5, 0), (1, 0, 3), (4, 1), (1, 0, 2), (2, 3), (2, 1), (1, 0, 1), (4, 2), (4, 3), (3, 2), (5, 2), (5, 1), (5, 3)),
-        (0, 1): ((1, 0, 1), (0, 0, 3), (0, 0, 2), (2, 2), (5, 1), (1, 0, 2), (2, 1), (3, 1), (4, 2), (2, 3), (4, 1), (5, 0), (4, 3), (5, 3), (3, 2), (5, 2)),
-        (1, 0): ((2, 2), (4, 0), (0, 0, 2), (2, 0), (0, 3, 0), (2, 3), (4, 2), (0, 0, 3), (5, 1), (1, 1, 3), (1, 0, 3), (1, 0, 2), (4, 3), (5, 2), (3, 0), (5, 0), (1, 2, 0)),
-        (1, 1): ((4, 0), (0, 1, 3), (2, 0), (3, 0), (4, 2), (0, 0, 3), (2, 2), (0, 3, 0), (0, 0, 2), (4, 3), (1, 0, 2), (1, 2, 0), (1, 1, 3), (5, 2), (1, 1, 2), (2, 3), (1, 3, 0), (3, 2), (5, 3)),
-        (2, 0): ((4, 3), (5, 1), (4, 1), (4, 0), (1, 2, 0), (5, 2), (1, 2, 1), (2, 0), (5, 0), (1, 3, 0), (0, 0, 3)),
-        (2, 1): ((0, 3, 0), (4, 1), (4, 0), (1, 2, 3), (5, 2), (4, 3), (0, 3, 1), (1, 3, 0), (0, 1, 3), (0, 0, 3), (2, 0), (5, 1), (3, 0), (5, 0)),
-        (3, 0): ((4, 1), (1, 3, 1), (5, 3), (2, 1), (4, 0), (2, 0), (5, 2), (1, 3, 2), (4, 2), (5, 0), (5, 1)),
-        (3, 1): ((1, 3, 2), (2, 2), (4, 2), (4, 1), (3, 0), (3, 2), (1, 3, 1), (4, 0), (2, 1), (2, 0), (5, 1), (5, 0)),
-    },
-    {
-        (1, 0): ((1, 1, 2),),
-        (2, 1): ((1, 3, 1),),
-    },
-    {
-        (1, 0): ((3, 2), (1, 3, 0), (5, 3)),
-        (2, 1): ((5, 3), (3, 3), (1, 1, 3)),
-    },
-    {
+        (1, 0): ((0, 1, 0),),
+        (1, 1): ((1, 1, 0), (0, 1, 0)),
+        (2, 0): ((0, 2, 1), (1, 2, 0), (0, 2, 0), (1, 2, 1)),
+        (2, 1): ((0, 2, 0), (1, 2, 0)),
+        (3, 0): ((0, 3, 2), (0, 3, 1), (0, 3, 0)),
+        (3, 1): ((0, 3, 2), (0, 3, 1)),
+    },
+    {
+        (0, 1): ((0, 0, 2),),
+        (1, 1): ((0, 1, 3),),
+        (2, 0): ((2, 3),),
+        (2, 1): ((2, 3), (0, 2, 1), (0, 2, 3)),
+        (3, 1): ((0, 3, 0),),
+    },
+    {
+        (0, 0): ((1, 0, 1),),
+        (1, 0): ((1, 1, 0), (0, 1, 2)),
+    },
+    {
+        (1, 0): ((1, 2, 0), (2, 2)),
+        (1, 1): ((0, 1, 2), (0, 2, 0)),
+        (2, 0): ((1, 2, 3), (0, 2, 3)),
+        (2, 1): ((0, 3, 1),),
+    },
+    {
+        (0, 0): ((0, 0, 1), (2, 1), (3, 1), (5, 0), (0, 0, 2), (0, 0, 3), (1, 0, 3), (5, 1), (2, 2), (4, 2), (1, 0, 2), (2, 3), (4, 1), (4, 3), (3, 2)),
+        (0, 1): ((1, 0, 3), (5, 0), (2, 1), (2, 2), (0, 0, 1), (0, 0, 3), (4, 1), (1, 0, 2), (1, 0, 1), (4, 2), (5, 2), (3, 2), (4, 3), (2, 3), (5, 1), (3, 1), (5, 3)),
+        (1, 0): ((3, 0), (4, 0), (0, 2, 0), (2, 0), (0, 1, 3), (4, 2), (0, 0, 2), (0, 3, 0), (3, 2), (0, 0, 3), (1, 0, 3), (1, 1, 3), (4, 3), (2, 3), (5, 3), (5, 0), (1, 0, 2), (1, 1, 2), (5, 2), (1, 3, 0)),
+        (1, 1): ((4, 0), (2, 2), (0, 0, 2), (2, 3), (1, 0, 3), (1, 2, 0), (2, 0), (4, 2), (0, 0, 3), (4, 3), (5, 1), (1, 0, 2), (5, 2), (1, 1, 3), (0, 3, 0), (3, 0), (5, 0), (5, 3), (1, 3, 0)),
+        (2, 0): ((4, 1), (0, 3, 0), (2, 1), (4, 3), (4, 0), (0, 1, 3), (5, 1), (0, 3, 1), (2, 0), (5, 0), (5, 3), (1, 3, 0), (0, 0, 3)),
+        (2, 1): ((1, 2, 3), (2, 1), (0, 1, 3), (4, 1), (4, 3), (0, 3, 0), (4, 0), (2, 0), (5, 1), (1, 3, 0), (1, 2, 1), (5, 3), (1, 0, 3), (5, 0), (3, 3), (0, 0, 3), (1, 3, 1), (5, 2), (3, 0)),
+        (3, 0): ((2, 2), (3, 2), (1, 3, 0), (5, 3), (1, 3, 2), (4, 1), (4, 0), (1, 3, 1), (2, 1), (4, 2), (5, 2), (2, 0), (5, 1), (5, 0)),
+        (3, 1): ((4, 2), (1, 3, 2), (2, 2), (1, 3, 0), (1, 3, 1), (4, 1), (2, 1), (3, 0), (4, 0), (5, 1), (5, 0), (2, 0), (3, 2)),
+    },
+    {
+        (0, 0): ((5, 2), (5, 3)),
+        (3, 0): ((3, 0),),
+    },
+    {
+        (2, 1): ((1, 1, 3),),
         (3, 1): ((5, 2),),
     },
-    {
-        (1, 1): ((5, 1), (5, 0)),
-        (2, 0): ((5, 3), (1, 1, 3)),
+    {},
+    {
+        (1, 1): ((1, 1, 2),),
+    },
+    {
+        (1, 0): ((3, 3), (5, 1)),
+        (2, 0): ((1, 3, 1), (3, 3)),
+    },
+    {
+        (0, 1): ((3, 3),),
+    },
+    {
+        (2, 0): ((1, 0, 3),),
+        (2, 1): ((3, 1),),
+        (3, 0): ((3, 1),),
+        (3, 1): ((5, 3), (3, 1)),
     },
     {
         (0, 0): ((3, 3),),
-        (2, 0): ((1, 0, 3), (1, 3, 1)),
-        (3, 1): ((5, 3),),
-    },
-    {},
-    {
-        (0, 1): ((3, 3),),
-        (3, 0): ((3, 0), (3, 1)),
-    },
-    {
-        (1, 0): ((3, 3),),
-        (2, 1): ((3, 1),),
-    },
-    {
-        (2, 0): ((3, 0), (3, 3)),
-        (3, 1): ((3, 1),),
-    },
-    {},
-    {
-        (0, 0): ((3, 1),),
-        (1, 1): ((3, 3),),
-    },
-    {},
-    {},
-    {},
-    {},
-    {},
-    {},
-    {},
+        (2, 0): ((5, 2),),
+    },
+    {
+        (1, 1): ((3, 2), (3, 3)),
+        (2, 0): ((1, 1, 3),),
+    },
+    {},
+    {},
+    {
+        (2, 0): ((3, 0),),
+    },
     {},
     {
         (2, 0): ((3, 1),),
     },
+    {},
+    {},
+    {},
+    {},
+    {},
+    {},
     {},
     {},
     {},
@@ -253,30 +250,30 @@
     ("await_near", 0),
     ("near", 0, 3),
     ("near", 0, 2),
-    ("settle", 0, 3),
-    ("near", 0, 1),
-    ("near", 0, 0),
     ("await_far", 1),
     ("far", 1, 3),
     ("far", 1, 2),
     ("cross", 1, 3),
-    ("settle", 0, 2),
+    ("settle", 0, 3),
     ("far", 1, 1),
     ("cross", 1, 2),
     ("far", 1, 0),
     ("cross", 1, 1),
     ("cross", 1, 0),
+    ("near", 0, 1),
+    ("near", 0, 0),
     ("await_near", 1),
     ("near", 1, 3),
     ("near", 1, 2),
-    ("settle", 0, 1),
     ("settle", 1, 3),
     ("near", 1, 1),
     ("near", 1, 0),
-    ("settle", 0, 0),
+    ("settle", 0, 2),
     ("settle", 1, 2),
     ("settle", 1, 1),
     ("settle", 1, 0),
+    ("settle", 0, 1),
+    ("settle", 0, 0),
 )
 
 WEIGHTS_IN, DOWN_IN, HAND_IN, HAND_DOWN, ROW, ACROSS = range(6)
@@ -744,13 +741,17 @@
             hid[k] = jnp.where(mine, hidden, 0.0).astype(jnp.bfloat16)
 
     core = t % 2
+    half_rows = rows // 2
     r1, r2, r3 = {}, {}, {}
     for k in everyone:
         for far in range(2):
             r1[k, far] = remote(c1.at[k, far], c1r.at[k, far], c_ss.at[0], c_rs.at[far, k], tp=cpeer)
-        r2[k] = remote(c2.at[k], c2r.at[k], c_ss.at[1], c_rs.at[2, k], tp=xpeer)
-        if k:
-            r3[k] = remote(c3.at[k], c3r.at[k], c_ss.at[2], c_rs.at[3, k], sp=flip(s, 1 if k == 3 else k))
+        for h in range(2):
+            some = pl.ds(h * half_rows, half_rows)
+            r2[k, h] = remote(c2.at[k, some], c2r.at[k, some], c_ss.at[1], c_rs.at[2 + h, k], tp=xpeer)
+            if k:
+                target = flip(s, 1 if k == 3 else k)
+                r3[k, h] = remote(c3.at[k, some], c3r.at[k, some], c_ss.at[2], c_rs.at[4 + h, k], sp=target)
 
     def block_of(wave, far):
         return 2 * ((1 - x) if far else x) + wave
@@ -773,25 +774,30 @@
         def _():
             with scoped(f"cross{wave}{k}"):
                 r1[k, 1].wait_recv()
-            c2[k] = (po[k, 1] + c1r[k, 1].astype(jnp.float32)).astype(jnp.bfloat16)
-            r2[k].start()
+            for h in range(2):
+                some = pl.ds(h * half_rows, half_rows)
+                c2[k, some] = (po[k, 1, some] + c1r[k, 1, some].astype(jnp.float32)).astype(jnp.bfloat16)
+                r2[k, h].start()
 
     def settle(wave, k):
         @pl.when(core == wave)
         def _():
             with scoped(f"settle{wave}{k}"):
                 r1[k, 0].wait_recv()
-                r2[k].wait_recv()
-            result = po[k, 0] + c1r[k, 0].astype(jnp.float32) + c2r[k].astype(jnp.float32)
-            if k == 2:
-                with scoped(f"pair{wave}"):
-                    r3[3].wait_recv()
-                result = result + c3r[3].astype(jnp.float32)
-            if k:
-                c3[k] = result.astype(jnp.bfloat16)
-                r3[k].start()
-            else:
-                po[0, 0] = result
+            for h in range(2):
+                some = pl.ds(h * half_rows, half_rows)
+                with scoped(f"settle{wave}{k}{h}"):
+                    r2[k, h].wait_recv()
+                result = po[k, 0, some] + c1r[k, 0, some].astype(jnp.float32) + c2r[k, some].astype(jnp.float32)
+                if k == 2:
+                    with scoped(f"pair{wave}{h}"):
+                        r3[3, h].wait_recv()
+                    result = result + c3r[3, some].astype(jnp.float32)
+                if k:
+                    c3[k, some] = result.astype(jnp.bfloat16)
+                    r3[k, h].start()
+                else:
+                    po[0, 0, some] = result
 
     for name, *where in TAIL:
         next_step()
@@ -808,12 +814,13 @@
                 await_weights((2,), block_of(where[0], name == "await_far"))
 
     next_step()
-    ffn = po[0, 0]
-    for k in (1, 2):
-        with scoped(f"r3_{k}"):
-            r3[k].wait_recv()
-        ffn = ffn + c3r[k].astype(jnp.float32)
-    out_ref[...] = (stream[...] + 0.5 * ffn).astype(jnp.bfloat16)
+    for h in range(2):
+        some = pl.ds(h * half_rows, half_rows)
+        for k in (1, 2):
+            with scoped(f"r3_{k}{h}"):
+                r3[k, h].wait_recv()
+        ffn = po[0, 0, some] + c3r[1, some].astype(jnp.float32) + c3r[2, some].astype(jnp.float32)
+        out_ref[some, :] = (stream[some, :] + 0.5 * ffn).astype(jnp.bfloat16)
 
     def sent(ref, sem):
         remote(ref, ref, sem, rs_rs.at[0], tp=cpeer).wait_send()
@@ -977,7 +984,7 @@
             dma((1,)),
             dma((2, n)),
             dma((3,)),
-            dma((4, n)),
+            dma((6, n)),
         ],
         compiler_params=pltpu.CompilerParams(
             collective_id=0, has_side_effects=True, vmem_limit_bytes=60 * 1024 * 1024

time: 95.8 us -> 92.8 us (0.969)
  Pallas kernels: 94 us -> 91.1 us
    pallas_call x1, Pallas kernels: 94 us -> 91.1 us  [one_device(): pl.pallas_call(functools.partial(layer_kernel, n, widths), out_shape=jax....]
where the time goes in v5:
time: 92.8 us; the launch traced here: 92.7 us
  Pallas kernels  91.1 us (98%)
  local copies, waits for them, and re-layouts  1.62 us (2%)
    pallas_call x1, Pallas kernels, one_device(): pl.pallas_call(functools.partial(layer_kernel, n, widths), out_shape=jax....  91.1 us

profile of v5, /device:TPU:1, one launch (start us, length us, event | category | flops | bytes accessed | tf_op | source)
XLA Modules:
  0.0 92.7 jit_solution(4800477249547825219)
XLA Ops:
  0.0 91.1 %shard_map.118 = bf16[192,512]{1,0:T(8,128)(2,1)} custom-call(bf16[192,128]{1,0:T(8,128)(2,1)} %q1_hbm.1, bf16[192,256]{1,0:T(8,128)(2,1)} %q2_hbm.1, bf16[192,128]{1,0:T(8,128)(2,1)} %k1_hbm.1, bf16[192,256]{1,0:T(8,128)(2,1)} %k2_hbm.1, bf16[192,2,128]{2,1,0:T(2,128)(2,1)} %v_hbm.1, f32[1,2]{1,0:T(1,128)} %bitcast.1, bf16[192,512]{1,0:T(8,128)(2,1)} %residual_hbm.1, ...), custom_call_target="tpu_custom_call" | custom-call | tf_op jit(solution)/shard_map/pallas_call | solution.py:925
  91.1 1.6 %copy.14 = bf16[192,512]{1,0:T(8,128)(2,1)} copy(bf16[192,512]{1,0:T(8,128)(2,1)} %shard_map.118) | data formatting | bytes 393216

commit v6 on v5

--- a/solution.py
+++ b/solution.py
@@ -390,9 +390,14 @@
 
     barrier = pltpu.get_barrier_semaphore()
     for k in others:
-        pl.semaphore_signal(barrier, inc=1, device_id={"sp": flip(s, k)}, device_id_type=pl.DeviceIdType.MESH)
         pl.semaphore_signal(barrier, inc=1, device_id={"tp": flip(t, k)}, device_id_type=pl.DeviceIdType.MESH)
     pl.semaphore_signal(barrier, inc=1, device_id={"grp": 1 - y}, device_id_type=pl.DeviceIdType.MESH)
+    for step, inside in ((1, s < last), (-1, s > 0)):
+
+        @pl.when(inside)
+        def _(step=step):
+            pl.semaphore_signal(barrier, inc=1, device_id={"sp": s + step}, device_id_type=pl.DeviceIdType.MESH)
+
     inputs = (
         (k1_hbm, k1_ref),
         (k2_hbm, k2_ref),
@@ -585,7 +590,8 @@
         load.wait()
     gains[t] = jnp.broadcast_to(gain_ref[...].reshape(1, blk), gains.shape[1:])
     with scoped("barrier"):
-        pl.semaphore_wait(barrier, 2 * (sp_count - 1) + 1)
+        ends = jnp.logical_or(s == 0, s == last)
+        pl.semaphore_wait(barrier, jnp.where(ends, sp_count + 1, sp_count + 2))
     next_step()
 
     @pl.when(s < last)

time: 92.8 us -> 91.8 us (0.989)
  Pallas kernels: 91.1 us -> 90.1 us
    pallas_call x1, Pallas kernels: 91.1 us -> 90.1 us  [one_device(): pl.pallas_call(functools.partial(layer_kernel, n, widths), out_shape=jax....]
where the time goes in v6:
time: 91.8 us; the launch traced here: 91.7 us
  Pallas kernels  90.1 us (98%)
  local copies, waits for them, and re-layouts  1.62 us (2%)
    pallas_call x1, Pallas kernels, one_device(): pl.pallas_call(functools.partial(layer_kernel, n, widths), out_shape=jax....  90.1 us

profile of v6, /device:TPU:1, one launch (start us, length us, event | category | flops | bytes accessed | tf_op | source)
XLA Modules:
  0.0 91.7 jit_solution(18394307460620833913)
XLA Ops:
  0.0 90.1 %shard_map.118 = bf16[192,512]{1,0:T(8,128)(2,1)} custom-call(bf16[192,128]{1,0:T(8,128)(2,1)} %q1_hbm.1, bf16[192,256]{1,0:T(8,128)(2,1)} %q2_hbm.1, bf16[192,128]{1,0:T(8,128)(2,1)} %k1_hbm.1, bf16[192,256]{1,0:T(8,128)(2,1)} %k2_hbm.1, bf16[192,2,128]{2,1,0:T(2,128)(2,1)} %v_hbm.1, f32[1,2]{1,0:T(1,128)} %bitcast.1, bf16[192,512]{1,0:T(8,128)(2,1)} %residual_hbm.1, ...), custom_call_target="tpu_custom_call" | custom-call | tf_op jit(solution)/shard_map/pallas_call | solution.py:931
  90.1 1.6 %copy.14 = bf16[192,512]{1,0:T(8,128)(2,1)} copy(bf16[192,512]{1,0:T(8,128)(2,1)} %shard_map.118) | data formatting | bytes 393216
